TPU v7x, 32 devices: a whole 2x2x4 slice. The times are simulated.
32 devices in a mesh: sp: 8 (over z, x), tp: 4 (over y, core).
Axes of the slice: x: 2, y: 2, z: 4, core: 2. Of those that a mesh axis runs over, the one named last changes fastest.
Arguments:
- query_one: bfloat16 [2048, 1024], P('sp', 'tp'), may hold values from -6 to 6
- key_one: bfloat16 [2048, 1024], P('sp', 'tp'), may hold values from -6 to 6
- value_one: bfloat16 [2048, 2048], P('sp', 'tp'), may hold values from -6 to 6
- gate_one: bfloat16 [2048, 2048], P('sp', 'tp'), may hold values from -6 to 6
- decay_one: float32 [2, 2048, 1024], P(None, 'sp', 'tp')
- query_two: bfloat16 [2048, 2048], P('sp', 'tp'), may hold values from -6 to 6
- key_two: bfloat16 [2048, 2048], P('sp', 'tp'), may hold values from -6 to 6
- value_two: bfloat16 [2048, 2048], P('sp', 'tp'), may hold values from -6 to 6
- gate_two: bfloat16 [2048, 2048], P('sp', 'tp'), may hold values from -6 to 6
- decay_two: float32 [2, 2048, 2048], P(None, 'sp', 'tp')
- head_gain: float32 [128], replicated, may hold values from 0.1 to 1.9
- proj_one: bfloat16 [2048, 2048], P('tp'), may hold values from -0.09375 to 0.09375
- proj_two: bfloat16 [2048, 2048], P('tp'), may hold values from -0.09375 to 0.09375
- stream: bfloat16 [2048, 2048], P('sp'), may hold values from -6 to 6
- gain_mix: float32 [2048], replicated, may hold values from 0.1 to 1.9
- gain_moe: float32 [2048], replicated, may hold values from 0.1 to 1.9
- routes: int32 [2048, 2], P('sp'), may hold values from 0 to 7, all different within a row; in each aligned block of 256 rows (0 to 255, 256 to 511, ...) at most 96 rows name the same one
- affinity: float32 [2048, 2], P('sp'), may hold values from 0.1 to 1
- expert_gate: bfloat16 [8, 2048, 2048], P('sp', None, 'tp'), may hold values from -0.125 to 0.125
- expert_up: bfloat16 [8, 2048, 2048], P('sp', None, 'tp'), may hold values from -0.125 to 0.125
- expert_down: bfloat16 [8, 2048, 2048], P('sp', 'tp'), may hold values from -0.125 to 0.125
Outputs:
- output: bfloat16 [2048, 2048], P(('sp', 'tp'))
Inputs may be any that keep to these rules, and one draw needn't show every extreme that they name: `routes`: in the 256 rows of one index of sp no expert is named more than 96 times, a bound that some block reaches there in every draw; a row names 2 different experts.
All inputs are finite; a program needn't handle non-finite values.
Results may differ from a plain program's by a relative error of at most 0.017.
Values may be sent and summed in bfloat16 or wider, within the bound.
A program may use at most 64 MiB of HBM per device.

v0:
```python
import functools

import jax
import jax.numpy as jnp
from jax import lax
from jax.experimental import pallas as pl
from jax.experimental.pallas import tpu as pltpu
from jax.sharding import PartitionSpec as P

DK_A = 64
DK_B = 128
BLK = 64
SHARPNESS = 16.0
F32 = jnp.float32
BF16 = jnp.bfloat16
MESH = pl.DeviceIdType.MESH
VMEM = pl.BlockSpec(memory_space=pltpu.VMEM)
DMA = pltpu.SemaphoreType.DMA


def params(collective_id=None):
    if collective_id is None:
        return pltpu.CompilerParams(vmem_limit_bytes=48 * 2**20)
    return pltpu.CompilerParams(
        vmem_limit_bytes=48 * 2**20, collective_id=collective_id, has_side_effects=True
    )


def mm(a, b):
    return jnp.dot(a, b, preferred_element_type=F32)


def mm_nt(a, b):
    return lax.dot_general(a, b, (((1,), (1,)), ((), ())), preferred_element_type=F32)


def mm_tn(a, b):
    return lax.dot_general(a, b, (((0,), (0,)), ((), ())), preferred_element_type=F32)


def log_sigmoid(x):
    return jnp.minimum(x, 0.0) - jnp.log1p(jnp.exp(-jnp.abs(x)))


def silu(x):
    return x / (1.0 + jnp.exp(-x))


def layer_norm(values, gain):
    mean = jnp.mean(values, axis=-1, keepdims=True)
    spread = jnp.mean(jnp.square(values - mean), axis=-1, keepdims=True)
    return (values - mean) * lax.rsqrt(spread + 1e-05) * gain


def greet(peers):
    barrier = pltpu.get_barrier_semaphore()
    for peer in peers:
        pl.semaphore_signal(barrier, inc=1, device_id=peer, device_id_type=MESH)
    pl.semaphore_wait(barrier, len(peers))


def remote(src, dst, send, recv, peer):
    return pltpu.make_async_remote_copy(
        src_ref=src, dst_ref=dst, send_sem=send, recv_sem=recv, device_id=peer, device_id_type=MESH
    )


def across(me, k, n):
    place, bit = 0, 1
    while bit < n:
        digit = lax.rem(me // bit, 2)
        place = place + (1 - digit if k & bit else digit) * bit
        bit *= 2
    return place


def state_kernel(ka, va, da, kb, vb, db, stack, cum):
    rows = ka.shape[0]
    count = rows // BLK
    ii = lax.broadcasted_iota(jnp.int32, (rows, rows), 0)
    jj = lax.broadcasted_iota(jnp.int32, (rows, rows), 1)
    same = (ii // BLK) == (jj // BLK)
    lower = jnp.where(same & (ii >= jj), 1.0, 0.0).astype(BF16)
    upper = jnp.where(same & (ii <= jj), 1.0, 0.0).astype(BF16)
    base = 0
    for k, v, d, dk in ((ka, va, da, DK_A), (kb, vb, db, DK_B)):
        wide = k.shape[1]
        heads = wide // dk
        dv = v.shape[1] // heads
        keys = k[...].astype(F32)
        for way in range(2):
            fade = log_sigmoid(d[way]) / SHARPNESS
            high = fade.astype(BF16)
            low = (fade - high.astype(F32)).astype(BF16)
            tri = lower if way == 0 else upper
            total = mm(tri, high) + mm(tri, low)
            cum[way, :, base : base + wide] = total
            tail = jnp.zeros((1, wide), F32)
            weighted = [None] * count
            for b in reversed(range(count)) if way == 0 else range(count):
                part = total[b * BLK : (b + 1) * BLK]
                last = part[BLK - 1 : BLK] if way == 0 else part[0:1]
                weighted[b] = (keys[b * BLK : (b + 1) * BLK] * jnp.exp(last - part + tail)).astype(BF16)
                tail = tail + last
            weighted = jnp.concatenate(weighted, axis=0)
            states = [
                mm_tn(v[:, h * dv : (h + 1) * dv], weighted[:, h * dk : (h + 1) * dk]).astype(BF16)
                for h in range(heads)
            ]
            states = states[0] if heads == 1 else jnp.concatenate(states, axis=1)
            thigh = tail.astype(BF16).astype(F32)
            row = lax.broadcasted_iota(jnp.int32, (16, wide), 0)
            fades = jnp.where(row == 0, thigh, jnp.where(row == 1, tail - thigh, 0.0)).astype(BF16)
            half = dv // 2
            for i in range(2):
                stack[i, way, 0:half, base : base + wide] = states[i * half : (i + 1) * half]
                stack[i, way, half : half + 16, base : base + wide] = fades
        base += wide


def spread(total, wide):
    row = lax.broadcasted_iota(jnp.int32, (16, wide), 0)
    high = total.astype(BF16).astype(F32)
    return jnp.where(row == 0, high, jnp.where(row == 1, total - high, 0.0)).astype(BF16)


def states_exchange_kernel(n, stack, out, xbox, agg, zbox, outbox, xs, xr, zs, zr, bs, br):
    me = lax.axis_index("sp")
    side = lax.rem(me, 2)
    pair = me // 2
    pairs = n // 2
    partner = me + 1 - 2 * side
    half = out.shape[2]
    lanes = out.shape[3]
    chunk = 256 if lanes % 256 == 0 else lanes
    count = lanes // chunk

    def pair_at(j):
        return lax.rem(pair + j, pairs)

    greet([{"sp": partner}] + [{"sp": pair_at(j) * 2 + side} for j in range(1, pairs)])

    def at(c):
        return pl.ds(c * chunk, chunk)

    def swap(c):
        return remote(
            stack.at[1 - side, :, :, at(c)], xbox.at[:, :, at(c)], xs.at[c], xr.at[c], {"sp": partner}
        )

    def along(c, j):
        way = jnp.where(pair_at(j) < pair, 1, 0)
        return remote(
            agg.at[way, :, at(c)], zbox.at[pair, :, at(c)], zs.at[c, j], zr.at[c, j],
            {"sp": pair_at(j) * 2 + side},
        )

    def back(c):
        return remote(
            outbox.at[:, :, at(c)], out.at[:, side, :, at(c)], bs.at[c], br.at[c], {"sp": partner}
        )

    for c in range(count):
        swap(c).start()
    zbox[pair] = jnp.zeros_like(zbox[pair])

    def load(ref, index, c):
        block = ref[index + (slice(None), at(c))].astype(F32)
        return block[0:half], block[half : half + 1] + block[half + 1 : half + 2]

    def both(c, way):
        own, own_fade = load(stack, (side, way), c)
        other, other_fade = load(xbox, (way,), c)
        low = side == 0
        return (
            jnp.where(low, own, other), jnp.where(low, own_fade, other_fade),
            jnp.where(low, other, own), jnp.where(low, other_fade, own_fade),
        )

    for c in range(count):
        swap(c).wait_recv()
        s0, t0, s1, t1 = both(c, 0)
        agg[0, 0:half, at(c)] = (jnp.exp(t1) * s0 + s1).astype(BF16)
        agg[0, half : half + 16, at(c)] = spread(t0 + t1, chunk)
        s0, t0, s1, t1 = both(c, 1)
        agg[1, 0:half, at(c)] = (jnp.exp(t0) * s1 + s0).astype(BF16)
        agg[1, half : half + 16, at(c)] = spread(t0 + t1, chunk)
        for j in range(1, pairs):
            along(c, j).start()
    for c in range(count):
        for j in range(1, pairs):
            along(c, j).wait_recv()
        ahead = jnp.zeros((half, chunk), F32)
        behind = jnp.zeros((half, chunk), F32)
        for s in range(pairs):
            state, fade = load(zbox, (s,), c)
            ahead = jnp.where(s < pair, jnp.exp(fade) * ahead + state, ahead)
        for s in reversed(range(pairs)):
            state, fade = load(zbox, (s,), c)
            behind = jnp.where(s > pair, jnp.exp(fade) * behind + state, behind)
        low = side == 0
        s0, t0, _, _ = both(c, 0)
        next_ahead = jnp.exp(t0) * ahead + s0
        _, _, s1, t1 = both(c, 1)
        next_behind = jnp.exp(t1) * behind + s1
        outbox[0, :, at(c)] = jnp.where(low, next_ahead, ahead).astype(BF16)
        outbox[1, :, at(c)] = jnp.where(low, behind, next_behind).astype(BF16)
        back(c).start()
        out[0, side, :, at(c)] = jnp.where(low, ahead, next_ahead).astype(BF16)
        out[1, side, :, at(c)] = jnp.where(low, next_behind, behind).astype(BF16)
    for c in range(count):
        swap(c).wait_send()
        for j in range(1, pairs):
            along(c, j).wait_send()
        back(c).wait_send()
        remote(
            outbox.at[:, :, at(c)], out.at[:, 1 - side, :, at(c)], bs.at[c], br.at[c], {"sp": partner}
        ).wait_recv()


def mix_kernel(states, cum, qa, ka, va, ga, qb, kb, vb, gb, gain, pa, pb, out, heads_ref):
    rows = qa.shape[0]
    count = rows // BLK
    dv = gain.shape[1]
    ii = lax.broadcasted_iota(jnp.int32, (BLK, BLK), 0)
    jj = lax.broadcasted_iota(jnp.int32, (BLK, BLK), 1)
    base = 0
    column = 0
    for q, k, v, g, dk in ((qa, ka, va, ga, DK_A), (qb, kb, vb, gb, DK_B)):
        heads = q.shape[1] // dk
        for h in range(heads):
            lanes = slice(base + h * dk, base + (h + 1) * dk)
            own = slice(h * dk, (h + 1) * dk)
            vown = slice(h * dv, (h + 1) * dv)
            forward = jnp.concatenate([states[0, i, :, lanes] for i in range(2)], axis=0).astype(F32)
            backward = jnp.concatenate([states[1, i, :, lanes] for i in range(2)], axis=0).astype(F32)
            mixed = [None] * count
            readers = [None] * count
            growth = [None] * count
            for b in range(count):
                at = slice(b * BLK, (b + 1) * BLK)
                query = q[at, own].astype(F32) * dk ** (-0.5)
                key = k[at, own].astype(F32)
                value = v[at, vown]
                cf = cum[0, at, lanes]
                cb = cum[1, at, lanes]
                qf = (query * jnp.exp(cf)).astype(BF16)
                kf = (key * jnp.exp(-cf)).astype(BF16)
                qr = (query * jnp.exp(cb)).astype(BF16)
                kr = (key * jnp.exp(-cb)).astype(BF16)
                scores = jnp.where(ii >= jj, mm_nt(qf, kf), 0.0) + jnp.where(ii <= jj, mm_nt(qr, kr), 0.0)
                inner = mm(scores.astype(BF16), value)
                lastf = cf[BLK - 1 : BLK]
                inner = inner + mm_nt(qf, forward.astype(BF16))
                if b < count - 1:
                    kfs = (key * jnp.exp(lastf - cf)).astype(BF16)
                    forward = jnp.exp(lastf) * forward + mm_tn(value, kfs)
                mixed[b] = inner
                readers[b] = qr
                lastb = cb[0:1]
                if b > 0:
                    kbs = (key * jnp.exp(lastb - cb)).astype(BF16)
                    growth[b] = (jnp.exp(lastb), mm_tn(value, kbs))
            for b in reversed(range(count)):
                at = slice(b * BLK, (b + 1) * BLK)
                whole = mixed[b] + mm_nt(readers[b], backward.astype(BF16))
                if b > 0:
                    backward = growth[b][0] * backward + growth[b][1]
                scale = lax.rsqrt(jnp.mean(whole * whole, axis=-1, keepdims=True) + 1e-06)
                heads_ref[at, column + h * dv : column + (h + 1) * dv] = (
                    whole * scale * gain[...] * silu(g[at, vown].astype(F32))
                ).astype(BF16)
        base += heads * dk
        column += heads * dv
    split = pa.shape[0]
    width = out.shape[1]
    tile = min(512, width)
    for j in range(width // tile):
        cols = slice(j * tile, (j + 1) * tile)
        out[:, cols] = (
            mm(heads_ref[:, :split], pa[:, cols]) + mm(heads_ref[:, split:], pb[:, cols])
        ).astype(BF16)


def settle_kernel(
    n, part, stream, gain, settled, columns, inbox, mid, midbox, outbox, cs, cr, ys, yr, send2, recv2
):
    me = lax.axis_index("tp")
    own = part.shape[0] // n
    wide = part.shape[1] // n
    core = lax.rem(me, 2)
    line = me // 2
    lines = n // 2
    greet([{"tp": lax.rem(me + k, n)} for k in range(1, n)])

    def rows_of(i):
        return pl.ds(pl.multiple_of(i * own, own), own)

    def cols_of(i):
        return pl.ds(pl.multiple_of(i * wide, wide), wide)

    def line_at(j):
        return lax.rem(line + j, lines)

    def to_core(j):
        i = line_at(j) * 2 + 1 - core
        return remote(
            part.at[rows_of(i), :], inbox.at[j], cs.at[j], cr.at[j], {"tp": me + 1 - 2 * core}
        )

    def to_line(j):
        return remote(mid.at[j], midbox.at[j], ys.at[j], yr.at[j], {"tp": line_at(j) * 2 + core})

    for j in reversed(range(lines)):
        to_core(j).start()
    for j in reversed(range(lines)):
        to_core(j).wait_recv()
        mine = part[rows_of(line_at(j) * 2 + core), :].astype(F32) + inbox[j].astype(F32)
        if j > 0:
            mid[j] = mine.astype(BF16)
            to_line(j).start()
        else:
            total = mine
    for j in range(1, lines):
        to_line(j).wait_recv()
        total = total + midbox[j].astype(F32)
    total = total.astype(BF16).astype(F32)
    value = layer_norm(stream[rows_of(me), :].astype(F32) + total, gain[...])
    settled[...] = value
    outbox[...] = value.astype(BF16)
    second = []
    for k in range(1, n):
        peer = lax.rem(me + k, n)
        copy = remote(
            outbox.at[:, cols_of(peer)], columns.at[rows_of(me), :], send2.at[k], recv2.at[k], {"tp": peer}
        )
        copy.start()
        second.append(copy)
    columns[rows_of(me), :] = outbox[:, cols_of(me)]
    for k in range(1, n):
        source = lax.rem(me + n - k, n)
        second[k - 1].wait_send()
        remote(
            outbox.at[:, cols_of(source)], columns.at[rows_of(source), :], send2.at[k], recv2.at[k], {"tp": source}
        ).wait_recv()
    for j in range(lines):
        to_core(j).wait_send()
        if j > 0:
            to_line(j).wait_send()


def slots_of(routes, capacity, experts):
    rows, top = routes.shape
    lane = lax.broadcasted_iota(jnp.int32, (rows, max(128, experts)), 1)
    hots = [routes[:, i : i + 1] == lane for i in range(top)]
    named = sum(jnp.where(h, 1.0, 0.0) for h in hots)
    ii = lax.broadcasted_iota(jnp.int32, (rows, rows), 0)
    jj = lax.broadcasted_iota(jnp.int32, (rows, rows), 1)
    before = mm(jnp.where(ii > jj, 1.0, 0.0).astype(BF16), named.astype(BF16))
    slots = []
    for i in range(top):
        rank = jnp.sum(jnp.where(hots[i], before, 0.0), axis=1, keepdims=True).astype(jnp.int32)
        slots.append(routes[:, i : i + 1] * capacity + rank)
    return slots


def pick_kernel(capacity, experts, routes, columns, out):
    slots = slots_of(routes[...], capacity, experts)
    rows = columns.shape[0]
    lane = lax.broadcasted_iota(jnp.int32, (rows, experts * capacity), 1)
    hot = sum(jnp.where(lane == s, 1.0, 0.0) for s in slots).astype(BF16)
    out[...] = mm_tn(hot, columns[...]).astype(BF16)


def dispatch_kernel(n, m, x, out, ss, sr, ys, yr, cs, cr, fs, fr, local):
    me = lax.axis_index("sp")
    my = lax.axis_index("tp")
    wide = x.shape[2]
    core = lax.rem(my, 2)
    line = my // 2
    lines = m // 2
    partner = my + 1 - 2 * core

    def cols_of(i):
        return pl.ds(pl.multiple_of(i * wide, wide), wide)

    def line_peer(j):
        return lax.rem(line + j, lines) * 2 + core

    def line_source(j):
        return lax.rem(line + lines - j, lines) * 2 + core

    greet(
        [{"sp": lax.rem(me + k, n)} for k in range(1, n)]
        + [{"tp": partner}]
        + [{"tp": line_peer(j)} for j in range(1, lines)]
    )

    def cross(k):
        peer = across(me, k, n)
        return remote(x.at[peer], out.at[me, :, cols_of(my)], ss.at[k], sr.at[k], {"sp": peer})

    for k in range(1, n):
        cross(k).start()
    own = pltpu.make_async_copy(x.at[me], out.at[me, :, cols_of(my)], local)
    own.start()

    def block(s, i):
        return out.at[s, :, cols_of(i)]

    def to_line(k, s, j, i):
        return remote(block(s, i), block(s, i), ys.at[k, j], yr.at[k, j], {"tp": line_peer(j)})

    def to_core(k, s, i):
        return remote(block(s, i), block(s, i), cs.at[k], cr.at[k], {"tp": partner})

    def forward(k, s, j, i):
        return remote(block(s, i), block(s, i), fs.at[k, j], fr.at[k, j], {"tp": partner})

    def source(k):
        return across(me, k, n)

    def hand_on(k, s):
        for j in range(1, lines):
            to_line(k, s, j, my).start()
        to_core(k, s, my).start()

    def pass_on(k, s):
        for j in range(1, lines):
            i = line_source(j)
            to_line(k, s, j, i).wait_recv()
            forward(k, s, j, i).start()

    own.wait()
    hand_on(0, me)
    for k in range(1, n):
        s = source(k)
        remote(x.at[0], block(s, my), ss.at[k], sr.at[k], {"sp": s}).wait_recv()
        hand_on(k, s)
        pass_on(k - 1, source(k - 1))
    pass_on(n - 1, source(n - 1))
    for k in range(n):
        s = source(k)
        if k > 0:
            cross(k).wait_send()
        to_core(k, s, my).wait_send()
        to_core(k, s, partner).wait_recv()
        for j in range(1, lines):
            i = line_source(j)
            to_line(k, s, j, my).wait_send()
            forward(k, s, j, i).wait_send()
            forward(k, s, j, i + 1 - 2 * core).wait_recv()


def return_kernel(n, m, x, out, inbox, mid, midbox, last, cs, cr, ys, yr, ss, sr):
    me = lax.axis_index("sp")
    my = lax.axis_index("tp")
    wide = out.shape[2]
    core = lax.rem(my, 2)
    line = my // 2
    lines = m // 2
    partner = my + 1 - 2 * core

    def cols_of(i):
        return pl.ds(pl.multiple_of(i * wide, wide), wide)

    def line_at(j):
        return lax.rem(line + j, lines)

    greet(
        [{"sp": lax.rem(me + k, n)} for k in range(1, n)]
        + [{"tp": partner}]
        + [{"tp": line_at(j) * 2 + core} for j in range(1, lines)]
    )

    def place(k):
        return across(me, n - 1 - k, n)

    def to_core(k, j):
        i = line_at(j) * 2 + 1 - core
        return remote(x.at[place(k), :, cols_of(i)], inbox.at[k, j], cs.at[k, j], cr.at[k, j], {"tp": partner})

    def to_line(k, j):
        return remote(
            mid.at[k, j], midbox.at[k, j], ys.at[k, j], yr.at[k, j], {"tp": line_at(j) * 2 + core}
        )

    def cross(k):
        peer = place(k)
        return remote(last.at[k], out.at[me], ss.at[k], sr.at[k], {"sp": peer})

    for k in range(n):
        for j in reversed(range(lines)):
            to_core(k, j).start()

    def first(k):
        for j in reversed(range(lines)):
            to_core(k, j).wait_recv()
            i = line_at(j) * 2 + core
            mine = x[place(k), :, cols_of(i)].astype(F32) + inbox[k, j].astype(F32)
            mid[k, j] = mine.astype(BF16)
            if j > 0:
                to_line(k, j).start()

    def second(k):
        total = mid[k, 0].astype(F32)
        for j in range(1, lines):
            to_line(k, j).wait_recv()
            total = total + midbox[k, j].astype(F32)
        if k < n - 1:
            last[k] = total.astype(BF16)
            cross(k).start()
        else:
            out[me] = total.astype(BF16)

    first(0)
    for k in range(1, n):
        first(k)
        second(k - 1)
    second(n - 1)
    for k in range(n):
        for j in range(lines):
            to_core(k, j).wait_send()
            if j > 0:
                to_line(k, j).wait_send()
        if k < n - 1:
            cross(k).wait_send()
            s = place(k)
            remote(last.at[k], out.at[s], ss.at[k], sr.at[k], {"sp": s}).wait_recv()


def finish_kernel(n, capacity, experts, routes, affinity, pieces, settled, gain, out, term, mixture, send, recv):
    me = lax.axis_index("tp")
    rows = routes.shape[0]
    own = rows // n
    wide = pieces.shape[1]
    greet([{"tp": lax.rem(me + k, n)} for k in range(1, n)])

    def rows_of(i):
        return pl.ds(pl.multiple_of(i * own, own), own)

    def cols_of(i):
        return pl.ds(pl.multiple_of(i * wide, wide), wide)

    slots = slots_of(routes[...], capacity, experts)
    weights = affinity[...] / jnp.sum(affinity[...], axis=-1, keepdims=True)
    lane = lax.broadcasted_iota(jnp.int32, (rows, experts * capacity), 1)
    total = jnp.zeros((rows, wide), F32)
    for i, slot in enumerate(slots):
        hot = jnp.where(lane == slot, 1.0, 0.0).astype(BF16)
        total = total + weights[:, i : i + 1] * mm(hot, pieces[...])
    term[...] = total.astype(BF16)
    copies = []
    for k in range(1, n):
        peer = lax.rem(me + k, n)
        copy = remote(term.at[rows_of(peer), :], mixture.at[:, cols_of(me)], send.at[k], recv.at[k], {"tp": peer})
        copy.start()
        copies.append(copy)
    mixture[:, cols_of(me)] = term[rows_of(me), :]
    for k in range(1, n):
        source = lax.rem(me + n - k, n)
        copies[k - 1].wait_send()
        remote(
            term.at[rows_of(source), :], mixture.at[:, cols_of(source)], send.at[k], recv.at[k], {"tp": source}
        ).wait_recv()
    out[...] = layer_norm(settled[...] + mixture[...].astype(F32), gain[...]).astype(BF16)


def call(kernel, outs, scratch, count, collective_id=None):
    single = not isinstance(outs, list)
    return pl.pallas_call(
        kernel,
        out_shape=outs,
        in_specs=[VMEM] * count,
        out_specs=VMEM if single else [VMEM] * len(outs),
        scratch_shapes=scratch,
        compiler_params=params(collective_id),
    )


def body(
    query_one,
    key_one,
    value_one,
    gate_one,
    decay_one,
    query_two,
    key_two,
    value_two,
    gate_two,
    decay_two,
    head_gain,
    proj_one,
    proj_two,
    stream,
    gain_mix,
    gain_moe,
    routes,
    affinity,
    expert_gate,
    expert_up,
    expert_down,
):
    shape = jax.ShapeDtypeStruct
    rows = query_one.shape[0]
    n = lax.axis_size("sp")
    m = lax.axis_size("tp")
    width = stream.shape[1]
    own = rows // m
    wide = width // m
    dv = head_gain.shape[0]
    lanes = query_one.shape[1] + query_two.shape[1]
    values = value_one.shape[1] + value_two.shape[1]
    local_experts = expert_gate.shape[0]
    experts = local_experts * n
    top = routes.shape[1]
    capacity = 3 * rows * top // (2 * experts)
    room = local_experts * capacity

    half = dv // 2
    stack, cum = call(
        state_kernel, [shape((2, 2, half + 16, lanes), BF16), shape((2, rows, lanes), F32)], [], 6
    )(key_one, value_one, decay_one, key_two, value_two, decay_two)
    chunks = max(1, lanes // 256)
    states = call(
        functools.partial(states_exchange_kernel, n),
        shape((2, 2, half, lanes), BF16),
        [
            pltpu.VMEM((2, half + 16, lanes), BF16),
            pltpu.VMEM((2, half + 16, lanes), BF16),
            pltpu.VMEM((n // 2, half + 16, lanes), BF16),
            pltpu.VMEM((2, half, lanes), BF16),
            DMA((chunks,)), DMA((chunks,)), DMA((chunks, n // 2)), DMA((chunks, n // 2)),
            DMA((chunks,)), DMA((chunks,)),
        ],
        1,
        1,
    )(stack)
    part = call(mix_kernel, shape((rows, width), BF16), [pltpu.VMEM((rows, values), BF16)], 13)(
        states, cum, query_one, key_one, value_one, gate_one, query_two, key_two, value_two, gate_two,
        head_gain.reshape(1, -1), proj_one, proj_two,
    )
    settled, columns = call(
        functools.partial(settle_kernel, m),
        [shape((own, width), F32), shape((rows, wide), BF16)],
        [pltpu.VMEM((m // 2, own, width), BF16)] * 3
        + [pltpu.VMEM((own, width), BF16)]
        + [DMA((m // 2,))] * 4
        + [DMA((m,))] * 2,
        3,
        2,
    )(part, stream, gain_mix.reshape(1, -1))
    outgoing = call(
        functools.partial(pick_kernel, capacity, experts), shape((experts * capacity, wide), BF16), [], 2
    )(routes, columns)
    lines = m // 2
    received = call(
        functools.partial(dispatch_kernel, n, m),
        shape((n, room, width), BF16),
        [DMA((n,)), DMA((n,)), DMA((n, lines)), DMA((n, lines)), DMA((n,)), DMA((n,)),
         DMA((n, lines)), DMA((n, lines)), DMA],
        1,
        3,
    )(outgoing.reshape(n, room, wide))
    x = received.reshape(n, local_experts, capacity, width)
    results = []
    for e in range(local_experts):
        xe = x[:, e].reshape(n * capacity, width)
        gate = mm(xe, expert_gate[e])
        upward = mm(xe, expert_up[e])
        act = (jax.nn.silu(gate) * upward).astype(BF16)
        results.append(mm(act, expert_down[e]).astype(BF16).reshape(n, capacity, width))
    partial_value = results[0] if local_experts == 1 else jnp.concatenate(results, axis=1)
    pieces = call(
        functools.partial(return_kernel, n, m),
        shape((n, room, wide), BF16),
        [pltpu.VMEM((n, lines, room, wide), BF16)] * 3
        + [pltpu.VMEM((n, room, wide), BF16)]
        + [DMA((n, lines))] * 4
        + [DMA((n,))] * 2,
        1,
        4,
    )(partial_value)
    return call(
        functools.partial(finish_kernel, m, capacity, experts),
        shape((own, width), BF16),
        [pltpu.VMEM((rows, wide), BF16), pltpu.VMEM((own, width), BF16), DMA((m,)), DMA((m,))],
        5,
        5,
    )(routes, affinity, pieces.reshape(experts * capacity, wide), settled, gain_moe.reshape(1, -1))


def solution(mesh):
    return jax.shard_map(
        body,
        mesh=mesh,
        in_specs=(
            P("sp", "tp"),
            P("sp", "tp"),
            P("sp", "tp"),
            P("sp", "tp"),
            P(None, "sp", "tp"),
            P("sp", "tp"),
            P("sp", "tp"),
            P("sp", "tp"),
            P("sp", "tp"),
            P(None, "sp", "tp"),
            P(),
            P("tp", None),
            P("tp", None),
            P("sp", None),
            P(),
            P(),
            P("sp", None),
            P("sp", None),
            P("sp", None, "tp"),
            P("sp", None, "tp"),
            P("sp", "tp", None),
        ),
        out_specs=P(("sp", "tp"), None),
        check_vma=False,
    )
```

profile of v0, /device:TPU:1, one launch (start us, length us, event | category | flops | bytes accessed | tf_op | source)
XLA Modules:
  0.0 137.6 jit_solution(16282343256616177120)
XLA Ops:
  0.0 0.0 copy-start
  0.0 1.1 copy-done.3
  1.1 0.9 copy-done.5
  2.1 0.9 copy-done.6
  3.0 1.2 copy-done.8
  4.2 0.9 copy-done.10
  5.1 1.0 copy-done.12
  6.2 0.0 copy-start.16
  6.2 0.0 copy-start.17
  6.2 0.0 copy-start.18
  6.2 0.0 copy-start.21
  6.2 2.5 %shard_map.199 = (bf16[2,2,80,768]{3,2,1,0:T(8,128)(2,1)S(1)}, f32[2,256,768]{2,1,0:T(8,128)S(1)}) custom-call(bf16[256,256]{1,0:T(8,128)(2,1)S(1)} %copy-done.10, bf16[256,512]{1,0:T(8,128)(2,1)S(1)} %copy-done.3, f32[2,256,256]{2,1,0:T(8,128)S(1)} %copy-done.12, bf16[256,512]{1,0:T(8,128)(2,1)S(1)} %copy-done.5, bf16[256,512]{1,0:T(8,128)(2,1)S(1)} %copy-done.6, ...), custom_call_target="tpu_custom_call" | custom-call | tf_op jit(solution)/shard_map/pallas_call | solution.py:621
  8.8 19.1 %shard_map.200.states = bf16[2,2,64,768]{3,2,1,0:T(8,128)(2,1)S(1)} custom-call(bf16[2,2,80,768]{3,2,1,0:T(8,128)(2,1)S(1)} %get-tuple-element.9.stack), custom_call_target="tpu_custom_call" | custom-call | tf_op jit(solution)/shard_map/pallas_call | solution.py:625
  27.9 0.0 copy-done.4
  27.9 0.0 copy-done.7
  27.9 0.0 copy-done.11
  27.9 0.0 copy-done.15
  27.9 0.0 copy-done.16
  27.9 0.0 copy-done.17
  27.9 0.0 copy-done.18
  27.9 0.0 copy-done.21
  27.9 0.0 copy-start.9
  28.0 0.0 copy-start.19
  28.0 9.8 %shard_map.201.part = bf16[256,2048]{1,0:T(8,128)(2,1)S(1)} custom-call(bf16[2,2,64,768]{3,2,1,0:T(8,128)(2,1)S(1)} %shard_map.200.states, f32[2,256,768]{2,1,0:T(8,128)S(1)} %get-tuple-element.10.cum, bf16[256,256]{1,0:T(8,128)(2,1)S(1)} %copy-done.18, bf16[256,256]{1,0:T(8,128)(2,1)S(1)} %copy-done.11, bf16[256,512]{1,0:T(8,128)(2,1)S(1)} %copy-done.4, ...), custom_call_target="tpu_custom_call" | custom-call | tf_op jit(solution)/shard_map/pallas_call | solution.py:639
  37.8 0.0 copy-start.22
  37.8 0.0 copy-done.9
  37.8 0.0 copy-done.19
  37.8 18.3 %shard_map.202 = (f32[64,2048]{1,0:T(8,128)S(1)}, bf16[256,512]{1,0:T(8,128)(2,1)S(1)}) custom-call(bf16[256,2048]{1,0:T(8,128)(2,1)S(1)} %shard_map.201.part, bf16[256,2048]{1,0:T(8,128)(2,1)S(1)} %copy-done.9, f32[1,2048]{1,0:T(1,128)S(1)} %bitcast.27), custom_call_target="tpu_custom_call" | custom-call | tf_op jit(solution)/shard_map/pallas_call | solution.py:643
  56.2 0.0 copy-start.13
  56.2 0.9 copy-done.13
  57.1 0.0 copy-done.22
  57.1 0.1 copy.23.routes
  57.2 1.0 shard_map.203
  58.2 0.0 copy-start.24
  58.2 28.9 %shard_map.204 = bf16[8,96,2048]{2,1,0:T(8,128)(2,1)S(1)} custom-call(bf16[8,96,512]{2,1,0:T(8,128)(2,1)S(1)} %bitcast.26), custom_call_target="tpu_custom_call" | custom-call | tf_op jit(solution)/shard_map/pallas_call | solution.py:657
  87.1 0.0 copy-start.1
  87.1 1.6 %copy-done.1 = bf16[8,96,2048]{2,1,0:T(8,128)(2,1)} copy-done((bf16[8,96,2048]{2,1,0:T(8,128)(2,1)}, bf16[8,96,2048]{2,1,0:T(8,128)(2,1)S(1)}, u32[]{:S(2)}) %copy-start.1) | copy-done | bytes 3145752
  88.7 0.0 copy-done.24
  88.7 2.9 %fusion.3 = f32[768,512]{1,0:T(8,128)} fusion(bf16[768,2048]{1,0:T(8,128)(2,1)S(1)} %bitcast.22, bf16[1,2048,512]{2,1,0:T(8,128)(2,1)S(1)} %copy-done.24), kind=kOutput, calls=%fused_computation.4 | convolution fusion | flops 1610612736 | bytes 6815744 | tf_op jit(solution)/shard_map/dot_general | solution.py:30
  91.6 8.1 %convolution_convert_fusion = bf16[768,2048]{1,0:T(8,128)(2,1)} fusion(bf16[1,512,2048]{2,1,0:T(8,128)(2,1)S(1)} %copy-done, f32[768,512]{1,0:T(8,128)} %fusion.3, bf16[768,2048]{1,0:T(8,128)(2,1)} %bitcast.23, bf16[1,2048,512]{2,1,0:T(8,128)(2,1)} %param.40), kind=kOutput, calls=%fused_computation | convolution fusion | flops 3225157632 | bytes 12058624 | tf_op jit(solution)/shard_map/dot_general | solution.py:30
  99.8 1.9 %copy-done.2 = bf16[768,2048]{1,0:T(8,128)(2,1)S(1)} copy-done((bf16[768,2048]{1,0:T(8,128)(2,1)S(1)}, bf16[768,2048]{1,0:T(8,128)(2,1)}, u32[]{:S(2)}) %copy-start.2) | copy-done | bytes 3145752
  101.7 26.1 %shard_map.205 = bf16[8,96,512]{2,1,0:T(8,128)(2,1)S(1)} custom-call(bf16[8,96,2048]{2,1,0:T(8,128)(2,1)S(1)} %bitcast.24), custom_call_target="tpu_custom_call" | custom-call | tf_op jit(solution)/shard_map/pallas_call | solution.py:674
  127.8 0.1 copy.24.affinity
  127.9 0.0 copy-done.20
  127.9 0.0 copy-start.14
  127.9 1.0 copy-done.14
  129.0 7.9 %shard_map.206 = bf16[64,2048]{1,0:T(8,128)(2,1)S(1)} custom-call(s32[256,2]{1,0:T(8,128)S(1)} %copy.23.routes, f32[256,2]{1,0:T(8,128)S(1)} %copy.24.affinity, bf16[768,512]{1,0:T(8,128)(2,1)S(1)} %bitcast.25, f32[64,2048]{1,0:T(8,128)S(1)} %copy-done.14, f32[1,2048]{1,0:T(1,128)S(1)} %bitcast.28), custom_call_target="tpu_custom_call" | custom-call | tf_op jit(solution)/shard_map/pallas_call | solution.py:684
  136.9 0.7 copy.26
  (15 shorter events, 0.0 us)
Async XLA Ops:
  0.0 91.6 %copy-start = (bf16[1,512,2048]{2,1,0:T(8,128)(2,1)S(1)}, bf16[1,512,2048]{2,1,0:T(8,128)(2,1)}, u32[]{:S(2)}) copy-start(bf16[1,512,2048]{2,1,0:T(8,128)(2,1)} %param.41) | copy-start | bytes 6291460
  0.0 1.1 copy-start.3
  1.1 0.9 copy-start.5
  2.1 0.9 copy-start.6
  3.0 1.2 copy-start.8
  4.2 0.9 copy-start.10
  5.1 1.0 copy-start.12
  6.2 21.7 %copy-start.4 = (bf16[256,512]{1,0:T(8,128)(2,1)S(1)}, bf16[256,512]{1,0:T(8,128)(2,1)}, u32[]{:S(2)}) copy-start(bf16[256,512]{1,0:T(8,128)(2,1)} %va.3) | copy-start | bytes 786436
  6.2 21.7 %copy-start.7 = (bf16[256,512]{1,0:T(8,128)(2,1)S(1)}, bf16[256,512]{1,0:T(8,128)(2,1)}, u32[]{:S(2)}) copy-start(bf16[256,512]{1,0:T(8,128)(2,1)} %vb.3) | copy-start | bytes 786436
  6.2 21.7 %copy-start.11 = (bf16[256,256]{1,0:T(8,128)(2,1)S(1)}, bf16[256,256]{1,0:T(8,128)(2,1)}, u32[]{:S(2)}) copy-start(bf16[256,256]{1,0:T(8,128)(2,1)} %ka.3) | copy-start | bytes 393220
  6.2 21.7 %copy-start.15 = (bf16[256,512]{1,0:T(8,128)(2,1)S(1)}, bf16[256,512]{1,0:T(8,128)(2,1)}, u32[]{:S(2)}) copy-start(bf16[256,512]{1,0:T(8,128)(2,1)} %ga.1) | copy-start | bytes 786436
  6.2 21.7 %copy-start.16 = (bf16[256,512]{1,0:T(8,128)(2,1)S(1)}, bf16[256,512]{1,0:T(8,128)(2,1)}, u32[]{:S(2)}) copy-start(bf16[256,512]{1,0:T(8,128)(2,1)} %qb.1) | copy-start | bytes 786436
  6.2 21.7 %copy-start.17 = (bf16[256,512]{1,0:T(8,128)(2,1)S(1)}, bf16[256,512]{1,0:T(8,128)(2,1)}, u32[]{:S(2)}) copy-start(bf16[256,512]{1,0:T(8,128)(2,1)} %gb.1) | copy-start | bytes 786436
  6.2 21.7 %copy-start.18 = (bf16[256,256]{1,0:T(8,128)(2,1)S(1)}, bf16[256,256]{1,0:T(8,128)(2,1)}, u32[]{:S(2)}) copy-start(bf16[256,256]{1,0:T(8,128)(2,1)} %qa.1) | copy-start | bytes 393220
  6.2 21.7 %copy-start.21 = (f32[128]{0:T(128)S(1)}, f32[128]{0:T(128)}, u32[]{:S(2)}) copy-start(f32[128]{0:T(128)} %param.31) | copy-start | bytes 1540
  27.9 9.9 %copy-start.9 = (bf16[256,2048]{1,0:T(8,128)(2,1)S(1)}, bf16[256,2048]{1,0:T(8,128)(2,1)}, u32[]{:S(2)}) copy-start(bf16[256,2048]{1,0:T(8,128)(2,1)} %stream.1) | copy-start | bytes 3145732
  28.0 9.9 %copy-start.19 = (f32[2048]{0:T(1024)S(1)}, f32[2048]{0:T(1024)}, u32[]{:S(2)}) copy-start(f32[2048]{0:T(1024)} %param.35) | copy-start | bytes 24580
  37.8 19.3 %copy-start.22 = (s32[256,2]{0,1:T(2,128)S(1)}, s32[256,2]{0,1:T(2,128)}, u32[]{:S(2)}) copy-start(s32[256,2]{0,1:T(2,128)} %param.37) | copy-start | bytes 6148
  56.2 0.9 copy-start.13
  58.2 30.5 %copy-start.24 = (bf16[1,2048,512]{2,1,0:T(8,128)(2,1)S(1)}, bf16[1,2048,512]{2,1,0:T(8,128)(2,1)}, u32[]{:S(2)}) copy-start(bf16[1,2048,512]{2,1,0:T(8,128)(2,1)} %param.39) | copy-start | bytes 6291460
  87.1 1.6 %copy-start.1 = (bf16[8,96,2048]{2,1,0:T(8,128)(2,1)}, bf16[8,96,2048]{2,1,0:T(8,128)(2,1)S(1)}, u32[]{:S(2)}) copy-start(bf16[8,96,2048]{2,1,0:T(8,128)(2,1)S(1)} %shard_map.204) | copy-start | bytes 9437188
  99.8 1.9 %copy-start.2 = (bf16[768,2048]{1,0:T(8,128)(2,1)S(1)}, bf16[768,2048]{1,0:T(8,128)(2,1)}, u32[]{:S(2)}) copy-start(bf16[768,2048]{1,0:T(8,128)(2,1)} %convolution_convert_fusion) | copy-start | bytes 9437188
  101.7 26.1 %copy-start.23 = (f32[256,2]{0,1:T(2,128)S(1)}, f32[256,2]{0,1:T(2,128)}, u32[]{:S(2)}) copy-start(f32[256,2]{0,1:T(2,128)} %param.38) | copy-start | bytes 6148
  101.7 26.2 %copy-start.20 = (f32[2048]{0:T(1024)S(1)}, f32[2048]{0:T(1024)}, u32[]{:S(2)}) copy-start(f32[2048]{0:T(1024)} %param.36) | copy-start | bytes 24580
  127.9 1.0 copy-start.14
where the time goes:
time: 138 us
  Pallas kernels  114 us (83%)
  local copies, waits for them, and re-layouts  12.6 us (9%)
  matrix products  11.1 us (8%)
    pallas_call x1, Pallas kernels, body(): call(functools.partial(dispatch_kernel, n, m), shape((n, room, width), BF...  28.9 us
    pallas_call x1, Pallas kernels, body(): call(functools.partial(return_kernel, n, m), shape((n, room, wide), BF16)...  26.1 us
    pallas_call x1, Pallas kernels, body(): call(functools.partial(states_exchange_kernel, n), shape((2, 2, half, lan...  19.1 us
    pallas_call x1, Pallas kernels, body(): call(functools.partial(settle_kernel, m), [shape((own, width), F32), shap...  18.3 us
    unnamed x53, local copies, waits for them, and re-layouts  12.6 us
    dot_general x2, matrix products, mm(): return jnp.dot(a, b, preferred_element_type=F32)  11.1 us
    pallas_call x1, Pallas kernels, body(): call(mix_kernel, shape((rows, width), BF16), [pltpu.VMEM((rows, values),...  9.83 us
    pallas_call x1, Pallas kernels, body(): call(functools.partial(finish_kernel, m, capacity, experts), shape((own,...  7.91 us

commit v1 on v0

--- a/solution.py
+++ b/solution.py
@@ -350,219 +350,247 @@
 
 
 def slots_of(routes, capacity, experts):
-    rows, top = routes.shape
-    lane = lax.broadcasted_iota(jnp.int32, (rows, max(128, experts)), 1)
-    hots = [routes[:, i : i + 1] == lane for i in range(top)]
+    top, rows = routes.shape
+    levels = -(-max(16, experts) // 16) * 16
+    level = lax.broadcasted_iota(jnp.int32, (levels, rows), 0)
+    hots = [routes[i : i + 1] == level for i in range(top)]
     named = sum(jnp.where(h, 1.0, 0.0) for h in hots)
     ii = lax.broadcasted_iota(jnp.int32, (rows, rows), 0)
     jj = lax.broadcasted_iota(jnp.int32, (rows, rows), 1)
-    before = mm(jnp.where(ii > jj, 1.0, 0.0).astype(BF16), named.astype(BF16))
+    before = mm(named.astype(BF16), jnp.where(ii < jj, 1.0, 0.0).astype(BF16))
     slots = []
     for i in range(top):
-        rank = jnp.sum(jnp.where(hots[i], before, 0.0), axis=1, keepdims=True).astype(jnp.int32)
-        slots.append(routes[:, i : i + 1] * capacity + rank)
+        rank = jnp.sum(jnp.where(hots[i], before, 0.0), axis=0, keepdims=True).astype(jnp.int32)
+        slots.append(routes[i : i + 1] * capacity + rank)
     return slots
 
 
-def pick_kernel(capacity, experts, routes, columns, out):
-    slots = slots_of(routes[...], capacity, experts)
-    rows = columns.shape[0]
-    lane = lax.broadcasted_iota(jnp.int32, (rows, experts * capacity), 1)
-    hot = sum(jnp.where(lane == s, 1.0, 0.0) for s in slots).astype(BF16)
-    out[...] = mm_tn(hot, columns[...]).astype(BF16)
-
-
-def dispatch_kernel(n, m, x, out, ss, sr, ys, yr, cs, cr, fs, fr, local):
+def experts_kernel(
+    n, m, capacity, routes, affinity, columns, settled, gain, gate_hbm, up_hbm, down_hbm, out,
+    wg, wu, wd, outgoing, x, part, inbox, mid, midbox, last, pieces, total, term, mixture,
+    loads, ss, sr, ys, yr, cs, cr, fs, fr, rcs, rcr, rys, ryr, rss, rsr, send, recv,
+):
     me = lax.axis_index("sp")
     my = lax.axis_index("tp")
-    wide = x.shape[2]
+    local = wg.shape[0]
+    room = x.shape[1]
+    experts = local * n
+    top, rows = routes.shape
+    wide = columns.shape[1]
+    own = rows // m
     core = lax.rem(my, 2)
     line = my // 2
     lines = m // 2
     partner = my + 1 - 2 * core
 
+    weights = [
+        pltpu.make_async_copy(src, dst, loads.at[i])
+        for i, (src, dst) in enumerate(((gate_hbm, wg), (up_hbm, wu), (down_hbm, wd)))
+    ]
+    for copy in weights:
+        copy.start()
+
+    greet(
+        [{"sp": lax.rem(me + k, n)} for k in range(1, n)] + [{"tp": lax.rem(my + k, m)} for k in range(1, m)]
+    )
+
     def cols_of(i):
         return pl.ds(pl.multiple_of(i * wide, wide), wide)
 
-    def line_peer(j):
-        return lax.rem(line + j, lines) * 2 + core
+    def rows_of(i):
+        return pl.ds(pl.multiple_of(i * own, own), own)
+
+    def line_at(j):
+        return lax.rem(line + j, lines)
 
     def line_source(j):
-        return lax.rem(line + lines - j, lines) * 2 + core
-
-    greet(
-        [{"sp": lax.rem(me + k, n)} for k in range(1, n)]
-        + [{"tp": partner}]
-        + [{"tp": line_peer(j)} for j in range(1, lines)]
-    )
+        return lax.rem(line + lines - j, lines)
+
+    def peer(k):
+        return across(me, k, n)
+
+    def block(k, i):
+        return x.at[k, :, cols_of(i)]
 
     def cross(k):
-        peer = across(me, k, n)
-        return remote(x.at[peer], out.at[me, :, cols_of(my)], ss.at[k], sr.at[k], {"sp": peer})
-
-    for k in range(1, n):
-        cross(k).start()
-    own = pltpu.make_async_copy(x.at[me], out.at[me, :, cols_of(my)], local)
-    own.start()
-
-    def block(s, i):
-        return out.at[s, :, cols_of(i)]
-
-    def to_line(k, s, j, i):
-        return remote(block(s, i), block(s, i), ys.at[k, j], yr.at[k, j], {"tp": line_peer(j)})
-
-    def to_core(k, s, i):
-        return remote(block(s, i), block(s, i), cs.at[k], cr.at[k], {"tp": partner})
-
-    def forward(k, s, j, i):
-        return remote(block(s, i), block(s, i), fs.at[k, j], fr.at[k, j], {"tp": partner})
-
-    def source(k):
-        return across(me, k, n)
-
-    def hand_on(k, s):
+        return remote(outgoing.at[k], block(k, my), ss.at[k], sr.at[k], {"sp": peer(k)})
+
+    def to_line(k, j, i):
+        return remote(block(k, i), block(k, i), ys.at[k, j], yr.at[k, j], {"tp": line_at(j) * 2 + core})
+
+    def to_core(k, i):
+        return remote(block(k, i), block(k, i), cs.at[k], cr.at[k], {"tp": partner})
+
+    def forward(k, j, i):
+        return remote(block(k, i), block(k, i), fs.at[k, j], fr.at[k, j], {"tp": partner})
+
+    def hand_on(k):
+        if k > 0:
+            cross(k).wait_recv()
         for j in range(1, lines):
-            to_line(k, s, j, my).start()
-        to_core(k, s, my).start()
-
-    def pass_on(k, s):
+            to_line(k, j, my).start()
+        to_core(k, my).start()
+
+    def pass_on(k):
         for j in range(1, lines):
-            i = line_source(j)
-            to_line(k, s, j, i).wait_recv()
-            forward(k, s, j, i).start()
-
-    own.wait()
-    hand_on(0, me)
-    for k in range(1, n):
-        s = source(k)
-        remote(x.at[0], block(s, my), ss.at[k], sr.at[k], {"sp": s}).wait_recv()
-        hand_on(k, s)
-        pass_on(k - 1, source(k - 1))
-    pass_on(n - 1, source(n - 1))
+            i = line_source(j) * 2 + core
+            to_line(k, j, i).wait_recv()
+            forward(k, j, i).start()
+
+    def arrive(k):
+        to_core(k, partner).wait_recv()
+        for j in range(1, lines):
+            forward(k, j, line_source(j) * 2 + 1 - core).wait_recv()
+
+    def back_core(k, j):
+        i = line_at(j) * 2 + 1 - core
+        return remote(part.at[k, :, cols_of(i)], inbox.at[k, j], rcs.at[k, j], rcr.at[k, j], {"tp": partner})
+
+    def back_line(k, j):
+        return remote(
+            mid.at[k, j], midbox.at[k, j], rys.at[k, j], ryr.at[k, j], {"tp": line_at(j) * 2 + core}
+        )
+
+    def back_cross(k):
+        return remote(last.at[k], pieces.at[k], rss.at[k], rsr.at[k], {"sp": peer(k)})
+
+    def back_start(k):
+        for j in reversed(range(lines)):
+            back_core(k, j).start()
+
+    def back_first(k):
+        for j in reversed(range(lines)):
+            back_core(k, j).wait_recv()
+            i = line_at(j) * 2 + core
+            mine = part[k, :, cols_of(i)].astype(F32) + inbox[k, j].astype(F32)
+            mid[k, j] = mine.astype(BF16)
+            if j > 0:
+                back_line(k, j).start()
+
+    def back_second(k):
+        value = mid[k, 0].astype(F32)
+        for j in range(1, lines):
+            back_line(k, j).wait_recv()
+            value = value + midbox[k, j].astype(F32)
+        if k > 0:
+            last[k] = value.astype(BF16)
+            back_cross(k).start()
+        else:
+            pieces[k] = value.astype(BF16)
+
+    slots = slots_of(routes[...], capacity, experts)
+    seat = lax.broadcasted_iota(jnp.int32, (room, rows), 0)
     for k in range(n):
-        s = source(k)
+        base = peer(k) * room
+        hot = sum(jnp.where(seat == s - base, 1.0, 0.0) for s in slots).astype(BF16)
+        picked = mm(hot, columns[...]).astype(BF16)
+        if k == 0:
+            x[0, :, cols_of(my)] = picked
+            hand_on(0)
+        else:
+            outgoing[k] = picked
+            cross(k).start()
+
+    share = affinity[...] / jnp.sum(affinity[...], axis=0, keepdims=True)
+    sheet = [s.astype(F32) for s in slots] + [share[i : i + 1] for i in range(top)]
+    level = lax.broadcasted_iota(jnp.int32, (8, rows), 0)
+    sheet = sum(jnp.where(level == i, r, 0.0) for i, r in enumerate(sheet)).T
+    total[...] = jnp.zeros_like(total)
+
+    def gather(k):
+        if k > 0:
+            back_cross(k).wait_recv()
+        seats = lax.broadcasted_iota(jnp.int32, (rows, capacity), 1).astype(F32)
+        value = total[...]
+        for e in range(local):
+            base = ((peer(k) * local + e) * capacity).astype(F32)
+            rank = jnp.full((rows, 1), -1.0, F32)
+            scale = jnp.zeros((rows, 1), F32)
+            for i in range(top):
+                at = sheet[:, i : i + 1] - base
+                here = (at >= 0.0) & (at < capacity)
+                rank = jnp.where(here, at, rank)
+                scale = jnp.where(here, sheet[:, top + i : top + i + 1], scale)
+            hot = jnp.where(seats == rank, 1.0, 0.0).astype(BF16)
+            value = value + scale * mm(hot, pieces[k, e * capacity : (e + 1) * capacity, :])
+        total[...] = value
+
+    def multiply(first, count):
+        for e in range(local):
+            at = slice(e * capacity, (e + 1) * capacity)
+            xe = [x[k, at, :] for k in range(first, first + count)]
+            xe = xe[0] if count == 1 else jnp.concatenate(xe, axis=0)
+            act = (silu(mm(xe, wg[e])) * mm(xe, wu[e])).astype(BF16)
+            width = x.shape[2]
+            tile = min(512, width)
+            for c in range(width // tile):
+                cols = slice(c * tile, (c + 1) * tile)
+                value = mm(act, wd[e, :, cols]).astype(BF16)
+                for k in range(count):
+                    part[first + k, at, cols] = value[k * capacity : (k + 1) * capacity]
+
+    group = 2 if n % 2 == 0 and capacity % 16 == 0 else 1
+    ahead = group + 1
+    for k in range(1, min(n, ahead + 1)):
+        hand_on(k)
+        pass_on(k - 1)
+    if n <= ahead:
+        pass_on(n - 1)
+    groups = n // group
+    for p in range(groups):
+        mine = range(p * group, (p + 1) * group)
+        for k in mine:
+            arrive(k)
+        if p == 0:
+            for copy in weights:
+                copy.wait()
+        multiply(p * group, group)
+        for k in mine:
+            back_start(k)
+        if p > 0:
+            for k in range((p - 1) * group, p * group):
+                back_second(k)
+        for k in mine:
+            if k + ahead < n:
+                pass_on(k + ahead)
+            if k + ahead + 1 < n:
+                hand_on(k + ahead + 1)
+            back_first(k)
+        if p > 1:
+            for k in range((p - 2) * group, (p - 1) * group):
+                gather(k)
+    for k in range((groups - 1) * group, n):
+        back_second(k)
+    for k in range(max(0, groups - 2) * group, n):
+        gather(k)
+    term[...] = total[...].astype(BF16)
+
+    def swap(k, source, target):
+        return remote(
+            term.at[rows_of(source), :], mixture.at[:, cols_of(target)], send.at[k], recv.at[k], {"tp": source}
+        )
+
+    for k in range(1, m):
+        swap(k, lax.rem(my + k, m), my).start()
+    mixture[:, cols_of(my)] = term[rows_of(my), :]
+    for k in range(n):
         if k > 0:
             cross(k).wait_send()
-        to_core(k, s, my).wait_send()
-        to_core(k, s, partner).wait_recv()
+            back_cross(k).wait_send()
+        to_core(k, my).wait_send()
         for j in range(1, lines):
-            i = line_source(j)
-            to_line(k, s, j, my).wait_send()
-            forward(k, s, j, i).wait_send()
-            forward(k, s, j, i + 1 - 2 * core).wait_recv()
-
-
-def return_kernel(n, m, x, out, inbox, mid, midbox, last, cs, cr, ys, yr, ss, sr):
-    me = lax.axis_index("sp")
-    my = lax.axis_index("tp")
-    wide = out.shape[2]
-    core = lax.rem(my, 2)
-    line = my // 2
-    lines = m // 2
-    partner = my + 1 - 2 * core
-
-    def cols_of(i):
-        return pl.ds(pl.multiple_of(i * wide, wide), wide)
-
-    def line_at(j):
-        return lax.rem(line + j, lines)
-
-    greet(
-        [{"sp": lax.rem(me + k, n)} for k in range(1, n)]
-        + [{"tp": partner}]
-        + [{"tp": line_at(j) * 2 + core} for j in range(1, lines)]
-    )
-
-    def place(k):
-        return across(me, n - 1 - k, n)
-
-    def to_core(k, j):
-        i = line_at(j) * 2 + 1 - core
-        return remote(x.at[place(k), :, cols_of(i)], inbox.at[k, j], cs.at[k, j], cr.at[k, j], {"tp": partner})
-
-    def to_line(k, j):
-        return remote(
-            mid.at[k, j], midbox.at[k, j], ys.at[k, j], yr.at[k, j], {"tp": line_at(j) * 2 + core}
-        )
-
-    def cross(k):
-        peer = place(k)
-        return remote(last.at[k], out.at[me], ss.at[k], sr.at[k], {"sp": peer})
-
-    for k in range(n):
-        for j in reversed(range(lines)):
-            to_core(k, j).start()
-
-    def first(k):
-        for j in reversed(range(lines)):
-            to_core(k, j).wait_recv()
-            i = line_at(j) * 2 + core
-            mine = x[place(k), :, cols_of(i)].astype(F32) + inbox[k, j].astype(F32)
-            mid[k, j] = mine.astype(BF16)
+            i = line_source(j) * 2 + core
+            to_line(k, j, my).wait_send()
+            forward(k, j, i).wait_send()
+        for j in range(lines):
+            back_core(k, j).wait_send()
             if j > 0:
-                to_line(k, j).start()
-
-    def second(k):
-        total = mid[k, 0].astype(F32)
-        for j in range(1, lines):
-            to_line(k, j).wait_recv()
-            total = total + midbox[k, j].astype(F32)
-        if k < n - 1:
-            last[k] = total.astype(BF16)
-            cross(k).start()
-        else:
-            out[me] = total.astype(BF16)
-
-    first(0)
-    for k in range(1, n):
-        first(k)
-        second(k - 1)
-    second(n - 1)
-    for k in range(n):
-        for j in range(lines):
-            to_core(k, j).wait_send()
-            if j > 0:
-                to_line(k, j).wait_send()
-        if k < n - 1:
-            cross(k).wait_send()
-            s = place(k)
-            remote(last.at[k], out.at[s], ss.at[k], sr.at[k], {"sp": s}).wait_recv()
-
-
-def finish_kernel(n, capacity, experts, routes, affinity, pieces, settled, gain, out, term, mixture, send, recv):
-    me = lax.axis_index("tp")
-    rows = routes.shape[0]
-    own = rows // n
-    wide = pieces.shape[1]
-    greet([{"tp": lax.rem(me + k, n)} for k in range(1, n)])
-
-    def rows_of(i):
-        return pl.ds(pl.multiple_of(i * own, own), own)
-
-    def cols_of(i):
-        return pl.ds(pl.multiple_of(i * wide, wide), wide)
-
-    slots = slots_of(routes[...], capacity, experts)
-    weights = affinity[...] / jnp.sum(affinity[...], axis=-1, keepdims=True)
-    lane = lax.broadcasted_iota(jnp.int32, (rows, experts * capacity), 1)
-    total = jnp.zeros((rows, wide), F32)
-    for i, slot in enumerate(slots):
-        hot = jnp.where(lane == slot, 1.0, 0.0).astype(BF16)
-        total = total + weights[:, i : i + 1] * mm(hot, pieces[...])
-    term[...] = total.astype(BF16)
-    copies = []
-    for k in range(1, n):
-        peer = lax.rem(me + k, n)
-        copy = remote(term.at[rows_of(peer), :], mixture.at[:, cols_of(me)], send.at[k], recv.at[k], {"tp": peer})
-        copy.start()
-        copies.append(copy)
-    mixture[:, cols_of(me)] = term[rows_of(me), :]
-    for k in range(1, n):
-        source = lax.rem(me + n - k, n)
-        copies[k - 1].wait_send()
-        remote(
-            term.at[rows_of(source), :], mixture.at[:, cols_of(source)], send.at[k], recv.at[k], {"tp": source}
-        ).wait_recv()
+                back_line(k, j).wait_send()
+    for k in range(1, m):
+        source = lax.rem(my + m - k, m)
+        swap(k, source, source).wait_recv()
+    for k in range(1, m):
+        swap(k, lax.rem(my + k, m), my).wait_send()
     out[...] = layer_norm(settled[...] + mixture[...].astype(F32), gain[...]).astype(BF16)
 
 
@@ -650,44 +678,29 @@
         3,
         2,
     )(part, stream, gain_mix.reshape(1, -1))
-    outgoing = call(
-        functools.partial(pick_kernel, capacity, experts), shape((experts * capacity, wide), BF16), [], 2
-    )(routes, columns)
     lines = m // 2
-    received = call(
-        functools.partial(dispatch_kernel, n, m),
-        shape((n, room, width), BF16),
-        [DMA((n,)), DMA((n,)), DMA((n, lines)), DMA((n, lines)), DMA((n,)), DMA((n,)),
-         DMA((n, lines)), DMA((n, lines)), DMA],
-        1,
-        3,
-    )(outgoing.reshape(n, room, wide))
-    x = received.reshape(n, local_experts, capacity, width)
-    results = []
-    for e in range(local_experts):
-        xe = x[:, e].reshape(n * capacity, width)
-        gate = mm(xe, expert_gate[e])
-        upward = mm(xe, expert_up[e])
-        act = (jax.nn.silu(gate) * upward).astype(BF16)
-        results.append(mm(act, expert_down[e]).astype(BF16).reshape(n, capacity, width))
-    partial_value = results[0] if local_experts == 1 else jnp.concatenate(results, axis=1)
-    pieces = call(
-        functools.partial(return_kernel, n, m),
-        shape((n, room, wide), BF16),
-        [pltpu.VMEM((n, lines, room, wide), BF16)] * 3
-        + [pltpu.VMEM((n, room, wide), BF16)]
-        + [DMA((n, lines))] * 4
-        + [DMA((n,))] * 2,
-        1,
-        4,
-    )(partial_value)
-    return call(
-        functools.partial(finish_kernel, m, capacity, experts),
-        shape((own, width), BF16),
-        [pltpu.VMEM((rows, wide), BF16), pltpu.VMEM((own, width), BF16), DMA((m,)), DMA((m,))],
-        5,
-        5,
-    )(routes, affinity, pieces.reshape(experts * capacity, wide), settled, gain_moe.reshape(1, -1))
+    tall = pltpu.VMEM((n, lines, room, wide), BF16)
+    flat = pltpu.VMEM((n, room, wide), BF16)
+    whole = pltpu.VMEM((n, room, width), BF16)
+    hbm = pl.BlockSpec(memory_space=pl.ANY)
+    return pl.pallas_call(
+        functools.partial(experts_kernel, n, m, capacity),
+        out_shape=shape((own, width), BF16),
+        in_specs=[VMEM] * 5 + [hbm] * 3,
+        out_specs=VMEM,
+        scratch_shapes=[
+            pltpu.VMEM(expert_gate.shape, BF16), pltpu.VMEM(expert_up.shape, BF16),
+            pltpu.VMEM(expert_down.shape, BF16),
+            flat, whole, whole, tall, tall, tall, flat, flat,
+            pltpu.VMEM((rows, wide), F32), pltpu.VMEM((rows, wide), BF16), pltpu.VMEM((own, width), BF16),
+            DMA((3,)), DMA((n,)), DMA((n,)), DMA((n, lines)), DMA((n, lines)), DMA((n,)), DMA((n,)),
+            DMA((n, lines)), DMA((n, lines)), DMA((n, lines)), DMA((n, lines)), DMA((n, lines)), DMA((n, lines)),
+            DMA((n,)), DMA((n,)), DMA((m,)), DMA((m,)),
+        ],
+        compiler_params=params(3),
+    )(
+        routes.T, affinity.T, columns, settled, gain_moe.reshape(1, -1), expert_gate, expert_up, expert_down
+    )
 
 
 def solution(mesh):

time: 138 us -> 119 us (0.86)
  matrix products: 11.1 us -> 0 us
  local copies, waits for them, and re-layouts: 12.6 us -> 6.81 us
  Pallas kernels: 114 us -> 111 us
    dot_general x2 -> x0, matrix products: 11.1 us -> none  [mm(): return jnp.dot(a, b, preferred_element_type=F32)]
    unnamed x53 -> x41, local copies, waits for them, and re-layouts: 12.6 us -> 6.81 us
    pallas_call x4 -> x1, Pallas kernels: 63.8 us -> 61.3 us  [body(): pl.pallas_call(functools.partial(experts_kernel, n, m, capacity), out_sha...]
where the time goes in v1:
time: 119 us; the launch traced here: 118 us
  Pallas kernels  111 us (93%)
  local copies, waits for them, and re-layouts  6.81 us (6%)
    pallas_call x1, Pallas kernels, body(): pl.pallas_call(functools.partial(experts_kernel, n, m, capacity), out_sha...  61.3 us
    pallas_call x1, Pallas kernels, body(): call(functools.partial(states_exchange_kernel, n), shape((2, 2, half, lan...  19.1 us
    pallas_call x1, Pallas kernels, body(): call(functools.partial(settle_kernel, m), [shape((own, width), F32), shap...  18.3 us
    pallas_call x1, Pallas kernels, body(): call(mix_kernel, shape((rows, width), BF16), [pltpu.VMEM((rows, values),...  9.91 us
    unnamed x41, local copies, waits for them, and re-layouts  6.81 us
    pallas_call x1, Pallas kernels, body(): call(state_kernel, [shape((2, 2, half + 16, lanes), BF16), shape((2, rows...  2.52 us

profile of v1, /device:TPU:1, one launch (start us, length us, event | category | flops | bytes accessed | tf_op | source)
XLA Modules:
  0.0 118.2 jit_solution(805233925834071897)
XLA Ops:
  0.0 0.0 copy-start.19
  0.0 0.0 copy-start.2
  0.0 1.0 copy-done.2
  1.0 0.0 copy-start.4
  1.0 0.9 copy-done.4
  1.9 0.0 copy-start.5
  1.9 0.9 copy-done.5
  2.9 0.0 copy-start.6
  2.9 1.2 %copy-done.6 = f32[2,256,512]{2,1,0:T(8,128)S(1)} copy-done((f32[2,256,512]{2,1,0:T(8,128)S(1)}, f32[2,256,512]{2,1,0:T(8,128)}, u32[]{:S(2)}) %copy-start.6) | copy-done | bytes 1048600
  4.1 0.0 copy-start.8
  4.1 0.9 copy-done.8
  5.0 0.0 copy-start.10
  5.0 1.0 copy-done.10
  6.0 0.0 copy-start.3
  6.0 0.0 copy-start.9
  6.0 0.0 copy-start.11
  6.0 0.0 copy-start.12
  6.1 0.0 copy-start.13
  6.1 0.0 copy-start.14
  6.1 2.5 %shard_map.199 = (bf16[2,2,80,768]{3,2,1,0:T(8,128)(2,1)S(1)}, f32[2,256,768]{2,1,0:T(8,128)S(1)}) custom-call(bf16[256,256]{1,0:T(8,128)(2,1)S(1)} %copy-done.8, bf16[256,512]{1,0:T(8,128)(2,1)S(1)} %copy-done.2, f32[2,256,256]{2,1,0:T(8,128)S(1)} %copy-done.10, bf16[256,512]{1,0:T(8,128)(2,1)S(1)} %copy-done.4, bf16[256,512]{1,0:T(8,128)(2,1)S(1)} %copy-done.5, ...), custom_call_target="tpu_custom_call" | custom-call | tf_op jit(solution)/shard_map/pallas_call | solution.py:649
  8.6 19.1 %shard_map.200.states = bf16[2,2,64,768]{3,2,1,0:T(8,128)(2,1)S(1)} custom-call(bf16[2,2,80,768]{3,2,1,0:T(8,128)(2,1)S(1)} %get-tuple-element.9.stack), custom_call_target="tpu_custom_call" | custom-call | tf_op jit(solution)/shard_map/pallas_call | solution.py:653
  27.7 0.0 copy-done.19
  27.7 0.0 copy-done.3
  27.7 0.0 copy-done.9
  27.7 0.0 copy-done.11
  27.7 0.0 copy-done.12
  27.8 0.0 copy-done.13
  27.8 0.0 copy-done.14
  27.8 0.0 copy-start.7
  27.8 0.0 copy-start.15
  27.8 0.0 copy-start.1
  27.8 0.0 copy-start.18
  27.8 9.9 %shard_map.201.part = bf16[256,2048]{1,0:T(8,128)(2,1)S(1)} custom-call(bf16[2,2,64,768]{3,2,1,0:T(8,128)(2,1)S(1)} %shard_map.200.states, f32[2,256,768]{2,1,0:T(8,128)S(1)} %get-tuple-element.10.cum, bf16[256,256]{1,0:T(8,128)(2,1)S(1)} %copy-done.14, bf16[256,256]{1,0:T(8,128)(2,1)S(1)} %copy-done.9, bf16[256,512]{1,0:T(8,128)(2,1)S(1)} %copy-done.3, ...), custom_call_target="tpu_custom_call" | custom-call | tf_op jit(solution)/shard_map/pallas_call | solution.py:667
  37.7 0.0 copy-done.7
  37.7 0.0 copy-done.15
  37.8 0.0 copy-start
  37.8 0.0 copy-start.16
  37.8 0.0 copy-start.17
  37.8 18.3 %shard_map.202 = (f32[64,2048]{1,0:T(8,128)S(1)}, bf16[256,512]{1,0:T(8,128)(2,1)S(1)}) custom-call(bf16[256,2048]{1,0:T(8,128)(2,1)S(1)} %shard_map.201.part, bf16[256,2048]{1,0:T(8,128)(2,1)S(1)} %copy-done.7, f32[1,2048]{1,0:T(1,128)S(1)} %bitcast.5), custom_call_target="tpu_custom_call" | custom-call | tf_op jit(solution)/shard_map/pallas_call | solution.py:671
  56.1 0.0 copy-done.1
  56.2 0.0 copy-done.18
  56.2 0.0 copy-done
  56.2 0.0 copy-done.16
  56.2 0.0 copy-done.17
  56.2 61.3 %shard_map.203 = bf16[64,2048]{1,0:T(8,128)(2,1)S(1)} custom-call(s32[2,256]{1,0:T(2,128)S(1)} %bitcast.7, f32[2,256]{1,0:T(2,128)S(1)} %bitcast.8, bf16[256,512]{1,0:T(8,128)(2,1)S(1)} %get-tuple-element.11.columns, f32[64,2048]{1,0:T(8,128)S(1)} %get-tuple-element.12.settled, f32[1,2048]{1,0:T(1,128)S(1)} %bitcast.6, bf16[1,2048,512]{2,1,0:T(8,128)(2,1)S(1)} %copy-done, ...), custom_call_target="tpu_custom_call" | custom-call | tf_op jit(solution)/shard_map/pallas_call | solution.py:686
  117.5 0.7 copy.23
Async XLA Ops:
  0.0 27.7 %copy-start.19 = (f32[128]{0:T(128)S(1)}, f32[128]{0:T(128)}, u32[]{:S(2)}) copy-start(f32[128]{0:T(128)} %param.31) | copy-start | bytes 1540
  0.0 1.0 copy-start.2
  1.0 0.9 copy-start.4
  1.9 0.9 copy-start.5
  2.9 1.2 %copy-start.6 = (f32[2,256,512]{2,1,0:T(8,128)S(1)}, f32[2,256,512]{2,1,0:T(8,128)}, u32[]{:S(2)}) copy-start(f32[2,256,512]{2,1,0:T(8,128)} %db.1) | copy-start | bytes 3145732
  4.1 0.9 copy-start.8
  5.0 1.0 copy-start.10
  6.0 21.7 %copy-start.3 = (bf16[256,512]{1,0:T(8,128)(2,1)S(1)}, bf16[256,512]{1,0:T(8,128)(2,1)}, u32[]{:S(2)}) copy-start(bf16[256,512]{1,0:T(8,128)(2,1)} %va.3) | copy-start | bytes 786436
  6.0 21.7 %copy-start.9 = (bf16[256,256]{1,0:T(8,128)(2,1)S(1)}, bf16[256,256]{1,0:T(8,128)(2,1)}, u32[]{:S(2)}) copy-start(bf16[256,256]{1,0:T(8,128)(2,1)} %ka.3) | copy-start | bytes 393220
  6.0 21.7 %copy-start.11 = (bf16[256,512]{1,0:T(8,128)(2,1)S(1)}, bf16[256,512]{1,0:T(8,128)(2,1)}, u32[]{:S(2)}) copy-start(bf16[256,512]{1,0:T(8,128)(2,1)} %ga.1) | copy-start | bytes 786436
  6.0 21.7 %copy-start.12 = (bf16[256,512]{1,0:T(8,128)(2,1)S(1)}, bf16[256,512]{1,0:T(8,128)(2,1)}, u32[]{:S(2)}) copy-start(bf16[256,512]{1,0:T(8,128)(2,1)} %qb.1) | copy-start | bytes 786436
  6.1 21.7 %copy-start.13 = (bf16[256,512]{1,0:T(8,128)(2,1)S(1)}, bf16[256,512]{1,0:T(8,128)(2,1)}, u32[]{:S(2)}) copy-start(bf16[256,512]{1,0:T(8,128)(2,1)} %gb.1) | copy-start | bytes 786436
  6.1 21.7 %copy-start.14 = (bf16[256,256]{1,0:T(8,128)(2,1)S(1)}, bf16[256,256]{1,0:T(8,128)(2,1)}, u32[]{:S(2)}) copy-start(bf16[256,256]{1,0:T(8,128)(2,1)} %qa.1) | copy-start | bytes 393220
  27.8 10.0 %copy-start.7 = (bf16[256,2048]{1,0:T(8,128)(2,1)S(1)}, bf16[256,2048]{1,0:T(8,128)(2,1)}, u32[]{:S(2)}) copy-start(bf16[256,2048]{1,0:T(8,128)(2,1)} %stream.1) | copy-start | bytes 3145732
  27.8 10.0 %copy-start.15 = (f32[2048]{0:T(1024)S(1)}, f32[2048]{0:T(1024)}, u32[]{:S(2)}) copy-start(f32[2048]{0:T(1024)} %param.35) | copy-start | bytes 24580
  27.8 28.4 %copy-start.1 = (bf16[1,2048,512]{2,1,0:T(8,128)(2,1)S(1)}, bf16[1,2048,512]{2,1,0:T(8,128)(2,1)}, u32[]{:S(2)}) copy-start(bf16[1,2048,512]{2,1,0:T(8,128)(2,1)} %up_hbm.1) | copy-start | bytes 6291460
  27.8 28.3 %copy-start.18 = (f32[256,2]{0,1:T(2,128)S(1)}, f32[256,2]{0,1:T(2,128)}, u32[]{:S(2)}) copy-start(f32[256,2]{0,1:T(2,128)} %param.38) | copy-start | bytes 6148
  37.8 18.4 %copy-start = (bf16[1,2048,512]{2,1,0:T(8,128)(2,1)S(1)}, bf16[1,2048,512]{2,1,0:T(8,128)(2,1)}, u32[]{:S(2)}) copy-start(bf16[1,2048,512]{2,1,0:T(8,128)(2,1)} %gate_hbm.1) | copy-start | bytes 6291460
  37.8 18.4 %copy-start.16 = (f32[2048]{0:T(1024)S(1)}, f32[2048]{0:T(1024)}, u32[]{:S(2)}) copy-start(f32[2048]{0:T(1024)} %param.36) | copy-start | bytes 24580
  37.8 18.4 %copy-start.17 = (s32[256,2]{0,1:T(2,128)S(1)}, s32[256,2]{0,1:T(2,128)}, u32[]{:S(2)}) copy-start(s32[256,2]{0,1:T(2,128)} %param.37) | copy-start | bytes 6148

commit v2 on v1

v2 whole, which is shorter than its diff:
```python
import functools

import jax
import jax.numpy as jnp
from jax import lax
from jax.experimental import pallas as pl
from jax.experimental.pallas import tpu as pltpu
from jax.sharding import PartitionSpec as P

DK_A = 64
DK_B = 128
BLK = 64
SHARPNESS = 16.0
F32 = jnp.float32
BF16 = jnp.bfloat16
MESH = pl.DeviceIdType.MESH
VMEM = pl.BlockSpec(memory_space=pltpu.VMEM)
DMA = pltpu.SemaphoreType.DMA


def params(collective_id):
    return pltpu.CompilerParams(
        vmem_limit_bytes=60 * 2**20, collective_id=collective_id, has_side_effects=True
    )


def mm(a, b):
    return jnp.dot(a, b, preferred_element_type=F32)


def mm_nt(a, b):
    return lax.dot_general(a, b, (((1,), (1,)), ((), ())), preferred_element_type=F32)


def mm_tn(a, b):
    return lax.dot_general(a, b, (((0,), (0,)), ((), ())), preferred_element_type=F32)


def log_sigmoid(x):
    return jnp.minimum(x, 0.0) - jnp.log1p(jnp.exp(-jnp.abs(x)))


def silu(x):
    return x / (1.0 + jnp.exp(-x))


def layer_norm(values, gain):
    mean = jnp.mean(values, axis=-1, keepdims=True)
    spread = jnp.mean(jnp.square(values - mean), axis=-1, keepdims=True)
    return (values - mean) * lax.rsqrt(spread + 1e-05) * gain


def remote(src, dst, send, recv, peer):
    return pltpu.make_async_remote_copy(
        src_ref=src, dst_ref=dst, send_sem=send, recv_sem=recv, device_id=peer, device_id_type=MESH
    )


def across(me, k, n):
    place, bit = 0, 1
    while bit < n:
        digit = lax.rem(me // bit, 2)
        place = place + (1 - digit if k & bit else digit) * bit
        bit *= 2
    return place


def mixer(n, m, refs, scratch, sems, gain, gain_mix, columns, settled):
    qa, ka, va, ga, da, qb, kb, vb, gb, db, pa, pb, stream = refs
    stack, xbox, agg, zbox, outbox, states, fades, xfade, pfade, zfade, cum, mixed, readers, heads_ref = scratch[:14]
    part, inbox, mid, midbox, outbox_mix = scratch[14:]
    loads, xs, xr, xfs, xfr, zs, zr, zfs, zfr, bs, br, cs, cr, ys, yr, send2, recv2 = sems
    start, ready = loads
    me = lax.axis_index("sp")
    my = lax.axis_index("tp")
    rows = qa.shape[0]
    count = rows // BLK
    dv = gain.shape[1]
    half = dv // 2
    lanes = stack.shape[3]
    groups = ((qa, ka, va, ga, da, DK_A), (qb, kb, vb, gb, db, DK_B))
    side = lax.rem(me, 2)
    pair = me // 2
    pairs = n // 2
    partner = me + 1 - 2 * side
    chunk = 128 if all(g[1].shape[1] % 128 == 0 for g in groups) else lanes
    chunks = lanes // chunk

    def pair_at(j):
        return lax.rem(pair + j, pairs)

    def at(c):
        return pl.ds(c * chunk, chunk)

    def swap(c):
        return (
            remote(stack.at[1 - side, :, :, at(c)], xbox.at[:, :, at(c)], xs.at[c], xr.at[c], {"sp": partner}),
            remote(fades.at[:, :, at(c)], xfade.at[:, :, at(c)], xfs.at[c], xfr.at[c], {"sp": partner}),
        )

    def along(c, j):
        way = jnp.where(pair_at(j) < pair, 1, 0)
        peer = {"sp": pair_at(j) * 2 + side}
        return (
            remote(agg.at[way, :, at(c)], zbox.at[pair, :, at(c)], zs.at[c, j], zr.at[c, j], peer),
            remote(pfade.at[way, :, at(c)], zfade.at[pair, :, at(c)], zfs.at[c, j], zfr.at[c, j], peer),
        )

    def back(c, to):
        return remote(outbox.at[:, :, at(c)], states.at[:, to, :, at(c)], bs.at[c], br.at[c], {"sp": partner})

    def state(g, base):
        _, k, v, _, d, dk = groups[g]
        ii = lax.broadcasted_iota(jnp.int32, (rows, rows), 0)
        jj = lax.broadcasted_iota(jnp.int32, (rows, rows), 1)
        same = (ii // BLK) == (jj // BLK)
        wide = k.shape[1]
        heads = wide // dk
        keys = k[...].astype(F32)
        for way in range(2):
            fade = log_sigmoid(d[way]) / SHARPNESS
            high = fade.astype(BF16)
            low = (fade - high.astype(F32)).astype(BF16)
            tri = jnp.where(same & (ii >= jj if way == 0 else ii <= jj), 1.0, 0.0).astype(BF16)
            total = mm(tri, high) + mm(tri, low)
            cum[way, :, base : base + wide] = total
            tail = jnp.zeros((1, wide), F32)
            weighted = [None] * count
            for b in reversed(range(count)) if way == 0 else range(count):
                piece = total[b * BLK : (b + 1) * BLK]
                final = piece[BLK - 1 : BLK] if way == 0 else piece[0:1]
                weighted[b] = (keys[b * BLK : (b + 1) * BLK] * jnp.exp(final - piece + tail)).astype(BF16)
                tail = tail + final
            weighted = jnp.concatenate(weighted, axis=0)
            out = [
                mm_tn(v[:, h * dv : (h + 1) * dv], weighted[:, h * dk : (h + 1) * dk]).astype(BF16)
                for h in range(heads)
            ]
            out = out[0] if heads == 1 else jnp.concatenate(out, axis=1)
            for i in range(2):
                stack[i, way, :, base : base + wide] = out[i * half : (i + 1) * half]
            fades[way, :, base : base + wide] = tail

    def local(g, h, base, column):
        q, k, v, _, _, dk = groups[g]
        ii = lax.broadcasted_iota(jnp.int32, (BLK, BLK), 0)
        jj = lax.broadcasted_iota(jnp.int32, (BLK, BLK), 1)
        span = slice(base + h * dk, base + (h + 1) * dk)
        own = slice(h * dk, (h + 1) * dk)
        vown = slice(h * dv, (h + 1) * dv)
        place = slice(column + h * dv, column + (h + 1) * dv)
        result = [None] * count
        reads = [None] * count
        growth = [None] * count
        forward = None
        passed = jnp.zeros((1, dk), F32)
        for b in range(count):
            bat = slice(b * BLK, (b + 1) * BLK)
            query = q[bat, own].astype(F32) * dk ** (-0.5)
            key = k[bat, own].astype(F32)
            value = v[bat, vown]
            cf = cum[0, bat, span]
            cb = cum[1, bat, span]
            grown = query * jnp.exp(cf)
            qf = grown.astype(BF16)
            kf = (key * jnp.exp(-cf)).astype(BF16)
            reads[b] = query * jnp.exp(cb)
            qr = reads[b].astype(BF16)
            kr = (key * jnp.exp(-cb)).astype(BF16)
            scores = jnp.where(ii >= jj, mm_nt(qf, kf), 0.0) + jnp.where(ii <= jj, mm_nt(qr, kr), 0.0)
            inner = mm(scores.astype(BF16), value)
            lastf = cf[BLK - 1 : BLK]
            if b > 0:
                inner = inner + mm_nt(qf, forward.astype(BF16))
            readers[0, bat, span] = qf if b == 0 else (grown * jnp.exp(passed)).astype(BF16)
            passed = passed + lastf
            if b < count - 1:
                kfs = (key * jnp.exp(lastf - cf)).astype(BF16)
                added = mm_tn(value, kfs)
                forward = added if b == 0 else jnp.exp(lastf) * forward + added
            result[b] = inner
            lastb = cb[0:1]
            growth[b] = (lastb, mm_tn(value, (key * jnp.exp(lastb - cb)).astype(BF16)) if b > 0 else None)
        backward = None
        passed = jnp.zeros((1, dk), F32)
        for b in reversed(range(count)):
            bat = slice(b * BLK, (b + 1) * BLK)
            whole = result[b]
            if b < count - 1:
                whole = whole + mm_nt(reads[b].astype(BF16), backward.astype(BF16))
            mixed[bat, place] = whole
            readers[1, bat, span] = (reads[b] * jnp.exp(passed)).astype(BF16)
            passed = passed + growth[b][0]
            if b > 0:
                added = growth[b][1]
                backward = added if b == count - 1 else jnp.exp(growth[b][0]) * backward + added

    def settle_head(g, h, base, column):
        _, _, _, gate, _, dk = groups[g]
        span = slice(base + h * dk, base + (h + 1) * dk)
        vown = slice(h * dv, (h + 1) * dv)
        place = slice(column + h * dv, column + (h + 1) * dv)
        whole = mixed[:, place]
        for way in range(2):
            whole = whole + mm_nt(
                readers[way, :, span], jnp.concatenate([states[way, i, :, span] for i in range(2)], axis=0)
            )
        scale = lax.rsqrt(jnp.mean(whole * whole, axis=-1, keepdims=True) + 1e-06)
        heads_ref[:, place] = (whole * scale * gain[...] * silu(gate[:, vown].astype(F32))).astype(BF16)

    def both(c, way):
        own = stack[side, way, :, at(c)].astype(F32)
        other = xbox[way, :, at(c)].astype(F32)
        own_fade = fades[way, :, at(c)]
        other_fade = xfade[way, :, at(c)]
        low = side == 0
        return (
            jnp.where(low, own, other), jnp.where(low, own_fade, other_fade),
            jnp.where(low, other, own), jnp.where(low, other_fade, own_fade),
        )

    def first(c):
        for copy in swap(c):
            copy.wait_recv()
        s0, t0, s1, t1 = both(c, 0)
        agg[0, :, at(c)] = (jnp.exp(t1) * s0 + s1).astype(BF16)
        pfade[0, :, at(c)] = t0 + t1
        s0, t0, s1, t1 = both(c, 1)
        agg[1, :, at(c)] = (jnp.exp(t0) * s1 + s0).astype(BF16)
        pfade[1, :, at(c)] = t0 + t1
        for j in range(1, pairs):
            for copy in along(c, j):
                copy.start()

    def second(c):
        for j in range(1, pairs):
            for copy in along(c, j):
                copy.wait_recv()
        ahead = jnp.zeros((half, chunk), F32)
        behind = jnp.zeros((half, chunk), F32)
        for s in range(pairs):
            ahead = jnp.where(
                s < pair, jnp.exp(zfade[s, :, at(c)]) * ahead + zbox[s, :, at(c)].astype(F32), ahead
            )
        for s in reversed(range(pairs)):
            behind = jnp.where(
                s > pair, jnp.exp(zfade[s, :, at(c)]) * behind + zbox[s, :, at(c)].astype(F32), behind
            )
        low = side == 0
        s0, t0, _, _ = both(c, 0)
        next_ahead = jnp.exp(t0) * ahead + s0
        _, _, s1, t1 = both(c, 1)
        next_behind = jnp.exp(t1) * behind + s1
        outbox[0, :, at(c)] = jnp.where(low, next_ahead, ahead).astype(BF16)
        outbox[1, :, at(c)] = jnp.where(low, behind, next_behind).astype(BF16)
        back(c, side).start()
        states[0, side, :, at(c)] = jnp.where(low, ahead, next_ahead).astype(BF16)
        states[1, side, :, at(c)] = jnp.where(low, next_behind, behind).astype(BF16)

    zbox[pair] = jnp.zeros_like(zbox[pair])
    zfade[pair] = jnp.zeros_like(zfade[pair])
    heads = []
    base = 0
    column = 0
    for g, (_, k, v, _, _, dk) in enumerate(groups):
        ready(g)
        state(g, base)
        for h in range(k.shape[1] // dk):
            heads.append((g, h, base, column))
        base += k.shape[1]
        column += v.shape[1]
    start()
    for c in range(chunks):
        for copy in swap(c):
            copy.start()
    ready(2)
    events = [functools.partial(first, c) for c in range(chunks)] + [
        functools.partial(second, c) for c in range(chunks)
    ]
    early = min(2, len(heads))
    for head in heads[:early]:
        local(*head)
    rest = heads[early:]
    span = max(1, len(events) - 2)
    done = 0
    for i, event in enumerate(events):
        event()
        while done < len(rest) and done * span < (i + 1) * len(rest):
            local(*rest[done])
            done += 1
    for head in rest[done:]:
        local(*head)
    ended = 0
    for c in range(chunks):
        back(c, 1 - side).wait_recv()
        while ended < len(heads):
            g, h, base, _ = heads[ended]
            if base + (h + 1) * groups[g][5] > (c + 1) * chunk:
                break
            settle_head(*heads[ended])
            ended += 1

    ready(3)
    own = rows // m
    wide = columns.shape[1]
    width = part.shape[1]
    tile = min(512, width)
    tiles = width // tile
    core = lax.rem(my, 2)
    line = my // 2
    lines = m // 2
    split = pa.shape[0]

    def rows_of(i):
        return pl.ds(pl.multiple_of(i * own, own), own)

    def cols_of(i):
        return pl.ds(pl.multiple_of(i * wide, wide), wide)

    def line_at(j):
        return lax.rem(line + j, lines)

    def to_core(j, t):
        i = line_at(j) * 2 + 1 - core
        cut = pl.ds(t * tile, tile)
        return remote(
            part.at[rows_of(i), cut], inbox.at[j, :, cut], cs.at[j, t], cr.at[j, t], {"tp": my + 1 - 2 * core}
        )

    def to_line(j, t):
        cut = pl.ds(t * tile, tile)
        return remote(
            mid.at[j, :, cut], midbox.at[j, :, cut], ys.at[j, t], yr.at[j, t], {"tp": line_at(j) * 2 + core}
        )

    def project(t):
        cut = slice(t * tile, (t + 1) * tile)
        part[:, cut] = (mm(heads_ref[:, :split], pa[:, cut]) + mm(heads_ref[:, split:], pb[:, cut])).astype(BF16)
        for j in reversed(range(lines)):
            to_core(j, t).start()

    def add_core(t):
        cut = slice(t * tile, (t + 1) * tile)
        for j in reversed(range(lines)):
            to_core(j, t).wait_recv()
            mine = part[rows_of(line_at(j) * 2 + core), cut].astype(F32) + inbox[j, :, cut].astype(F32)
            if j > 0:
                mid[j, :, cut] = mine.astype(BF16)
                to_line(j, t).start()
            else:
                settled[:, cut] = mine

    def add_line(t):
        cut = slice(t * tile, (t + 1) * tile)
        value = settled[:, cut]
        for j in range(1, lines):
            to_line(j, t).wait_recv()
            value = value + midbox[j, :, cut].astype(F32)
        settled[:, cut] = stream[:, cut].astype(F32) + value.astype(BF16).astype(F32)

    for t in range(tiles):
        project(t)
        if t > 1:
            add_core(t - 2)
    for t in range(max(0, tiles - 2), tiles):
        add_core(t)
    for t in range(tiles):
        add_line(t)
    value = layer_norm(settled[...], gain_mix[...])
    settled[...] = value
    outbox_mix[...] = value.astype(BF16)

    def second_copy(k, source, target, peer):
        return remote(
            outbox_mix.at[:, cols_of(target)], columns.at[rows_of(source), :], send2.at[k], recv2.at[k], {"tp": peer}
        )

    order = [k for k in range(1, m) if k % 2 == 0] + [k for k in range(1, m) if k % 2 == 1]
    for k in order:
        peer = lax.rem(my + k, m)
        second_copy(k, my, peer, peer).start()
    columns[rows_of(my), :] = outbox_mix[:, cols_of(my)]
    for c in range(chunks):
        for copy in swap(c):
            copy.wait_send()
        for j in range(1, pairs):
            for copy in along(c, j):
                copy.wait_send()
        back(c, side).wait_send()
    for t in range(tiles):
        for j in range(lines):
            to_core(j, t).wait_send()
            if j > 0:
                to_line(j, t).wait_send()
    for k in range(1, m):
        source = lax.rem(my + m - k, m)
        second_copy(k, source, source, source).wait_recv()
    for k in range(1, m):
        peer = lax.rem(my + k, m)
        second_copy(k, my, peer, peer).wait_send()


def slots_of(routes, capacity, experts):
    top, rows = routes.shape
    levels = -(-max(16, experts) // 16) * 16
    level = lax.broadcasted_iota(jnp.int32, (levels, rows), 0)
    hots = [routes[i : i + 1] == level for i in range(top)]
    named = sum(jnp.where(h, 1.0, 0.0) for h in hots)
    ii = lax.broadcasted_iota(jnp.int32, (rows, rows), 0)
    jj = lax.broadcasted_iota(jnp.int32, (rows, rows), 1)
    before = mm(named.astype(BF16), jnp.where(ii < jj, 1.0, 0.0).astype(BF16))
    slots = []
    for i in range(top):
        rank = jnp.sum(jnp.where(hots[i], before, 0.0), axis=0, keepdims=True).astype(jnp.int32)
        slots.append(routes[i : i + 1] * capacity + rank)
    return slots


def experts_phase(n, m, capacity, routes, affinity, columns, settled, gain, weights, out, scratch, sems):
    wg, wu, wd, outgoing, x, part, inbox, mid, midbox, last, pieces, total, term, mixture = scratch
    ss, sr, ys, yr, cs, cr, fs, fr, rcs, rcr, rys, ryr, rss, rsr, send, recv = sems
    me = lax.axis_index("sp")
    my = lax.axis_index("tp")
    local = wg.shape[0]
    room = x.shape[1]
    experts = local * n
    top, rows = routes.shape
    wide = columns.shape[1]
    own = rows // m
    core = lax.rem(my, 2)
    line = my // 2
    lines = m // 2
    partner = my + 1 - 2 * core

    def cols_of(i):
        return pl.ds(pl.multiple_of(i * wide, wide), wide)

    def rows_of(i):
        return pl.ds(pl.multiple_of(i * own, own), own)

    def line_at(j):
        return lax.rem(line + j, lines)

    def line_source(j):
        return lax.rem(line + lines - j, lines)

    def peer(k):
        return across(me, k, n)

    def block(k, i):
        return x.at[k, :, cols_of(i)]

    def cross(k):
        return remote(outgoing.at[k], block(k, my), ss.at[k], sr.at[k], {"sp": peer(k)})

    def to_line(k, j, i):
        return remote(block(k, i), block(k, i), ys.at[k, j], yr.at[k, j], {"tp": line_at(j) * 2 + core})

    def to_core(k, i):
        return remote(block(k, i), block(k, i), cs.at[k], cr.at[k], {"tp": partner})

    def forward(k, j, i):
        return remote(block(k, i), block(k, i), fs.at[k, j], fr.at[k, j], {"tp": partner})

    def hand_on(k):
        if k > 0:
            cross(k).wait_recv()
        for j in range(1, lines):
            to_line(k, j, my).start()
        to_core(k, my).start()

    def pass_on(k):
        for j in range(1, lines):
            i = line_source(j) * 2 + core
            to_line(k, j, i).wait_recv()
            forward(k, j, i).start()

    def arrive(k):
        to_core(k, partner).wait_recv()
        for j in range(1, lines):
            forward(k, j, line_source(j) * 2 + 1 - core).wait_recv()

    def back_core(k, j):
        i = line_at(j) * 2 + 1 - core
        return remote(part.at[k, :, cols_of(i)], inbox.at[k, j], rcs.at[k, j], rcr.at[k, j], {"tp": partner})

    def back_line(k, j):
        return remote(
            mid.at[k, j], midbox.at[k, j], rys.at[k, j], ryr.at[k, j], {"tp": line_at(j) * 2 + core}
        )

    def back_cross(k):
        return remote(last.at[k], pieces.at[k], rss.at[k], rsr.at[k], {"sp": peer(k)})

    def back_start(k):
        for j in reversed(range(lines)):
            back_core(k, j).start()

    def back_first(k):
        for j in reversed(range(lines)):
            back_core(k, j).wait_recv()
            i = line_at(j) * 2 + core
            mine = part[k, :, cols_of(i)].astype(F32) + inbox[k, j].astype(F32)
            mid[k, j] = mine.astype(BF16)
            if j > 0:
                back_line(k, j).start()

    def back_second(k):
        value = mid[k, 0].astype(F32)
        for j in range(1, lines):
            back_line(k, j).wait_recv()
            value = value + midbox[k, j].astype(F32)
        if k > 0:
            last[k] = value.astype(BF16)
            back_cross(k).start()
        else:
            pieces[k] = value.astype(BF16)

    slots = slots_of(routes[...], capacity, experts)
    seat = lax.broadcasted_iota(jnp.int32, (room, rows), 0)
    far = list(range(n // 2, n - n // 4))
    near = [k for k in range(1, n) if k not in far]
    order = [0] + near[:1]
    for i in range(1, n):
        order += far[i - 1 : i] + near[i : i + 1]
    for k in order:
        base = peer(k) * room
        hot = sum(jnp.where(seat == s - base, 1.0, 0.0) for s in slots).astype(BF16)
        picked = mm(hot, columns[...]).astype(BF16)
        if k == 0:
            x[0, :, cols_of(my)] = picked
            hand_on(0)
        else:
            outgoing[k] = picked
            cross(k).start()

    share = affinity[...] / jnp.sum(affinity[...], axis=0, keepdims=True)
    sheet = [s.astype(F32) for s in slots] + [share[i : i + 1] for i in range(top)]
    level = lax.broadcasted_iota(jnp.int32, (8, rows), 0)
    sheet = sum(jnp.where(level == i, r, 0.0) for i, r in enumerate(sheet)).T
    total[...] = jnp.zeros_like(total)

    def gather(k):
        if k > 0:
            back_cross(k).wait_recv()
        seats = lax.broadcasted_iota(jnp.int32, (rows, capacity), 1).astype(F32)
        value = total[...]
        for e in range(local):
            base = ((peer(k) * local + e) * capacity).astype(F32)
            rank = jnp.full((rows, 1), -1.0, F32)
            scale = jnp.zeros((rows, 1), F32)
            for i in range(top):
                at = sheet[:, i : i + 1] - base
                here = (at >= 0.0) & (at < capacity)
                rank = jnp.where(here, at, rank)
                scale = jnp.where(here, sheet[:, top + i : top + i + 1], scale)
            hot = jnp.where(seats == rank, 1.0, 0.0).astype(BF16)
            value = value + scale * mm(hot, pieces[k, e * capacity : (e + 1) * capacity, :])
        total[...] = value

    def multiply(ks):
        for e in range(local):
            at = slice(e * capacity, (e + 1) * capacity)
            xe = [x[k, at, :] for k in ks]
            xe = xe[0] if len(xe) == 1 else jnp.concatenate(xe, axis=0)
            act = (silu(mm(xe, wg[e])) * mm(xe, wu[e])).astype(BF16)
            width = x.shape[2]
            tile = min(512, width)
            for c in range(width // tile):
                cols = slice(c * tile, (c + 1) * tile)
                value = mm(act, wd[e, :, cols]).astype(BF16)
                for i, k in enumerate(ks):
                    part[k, at, cols] = value[i * capacity : (i + 1) * capacity]

    group = 2 if n % 2 == 0 and capacity % 16 == 0 else 1
    handed = [0]
    passed = [-1]

    def hand_to(i):
        while handed[0] < min(i, n - 1):
            handed[0] += 1
            hand_on(order[handed[0]])

    def pass_to(i):
        while passed[0] < min(i, n - 1):
            hand_to(passed[0] + 1)
            passed[0] += 1
            pass_on(order[passed[0]])

    line_up = order[1:] + order[:1]
    sets = [line_up[i : i + group] for i in range(0, n, group)]
    hand_to(1)
    pass_to(0)
    hand_to(2)
    pass_to(1)
    hand_to(4)
    pass_to(2)
    hand_to(5)
    for p, ks in enumerate(sets):
        pass_to(group * (p + 1))
        for k in ks:
            arrive(k)
        if p == 0:
            for copy in weights:
                copy.wait()
        multiply(ks)
        for k in ks:
            back_start(k)
        pass_to(group * (p + 1) + 1)
        hand_to(group * (p + 1) + 4)
        if p > 1:
            for k in sets[p - 2]:
                back_second(k)
        for k in ks:
            back_first(k)
        hand_to(group * (p + 1) + 5)
        pass_to(group * (p + 2))
        if p > 2:
            for k in sets[p - 3]:
                gather(k)
    late = max(0, len(sets) - 2)
    for k in sets[late]:
        back_second(k)
    for p in range(max(0, len(sets) - 3), late):
        for k in sets[p]:
            gather(k)
    for p in range(late + 1, len(sets)):
        for k in sets[p]:
            back_second(k)
    for k in sets[late] + [k for ks in sets[late + 1 :] for k in reversed(ks)]:
        gather(k)
    term[...] = total[...].astype(BF16)

    def swap(k, source, target):
        return remote(
            term.at[rows_of(source), :], mixture.at[:, cols_of(target)], send.at[k], recv.at[k], {"tp": source}
        )

    for k in range(1, m):
        swap(k, lax.rem(my + k, m), my).start()
    mixture[:, cols_of(my)] = term[rows_of(my), :]
    for k in range(n):
        if k > 0:
            cross(k).wait_send()
            back_cross(k).wait_send()
        to_core(k, my).wait_send()
        for j in range(1, lines):
            i = line_source(j) * 2 + core
            to_line(k, j, my).wait_send()
            forward(k, j, i).wait_send()
        for j in range(lines):
            back_core(k, j).wait_send()
            if j > 0:
                back_line(k, j).wait_send()
    for k in range(1, m):
        source = lax.rem(my + m - k, m)
        swap(k, source, source).wait_recv()
    for k in range(1, m):
        swap(k, lax.rem(my + k, m), my).wait_send()
    out[...] = layer_norm(settled[...] + mixture[...].astype(F32), gain[...]).astype(BF16)


def layer_kernel(n, m, capacity, *refs):
    routes, affinity, gain, gain_mix, gain_moe = refs[:5]
    hbm = refs[5:21]
    out = refs[21]
    held = refs[22:38]
    rest = refs[38:]
    columns, settled = rest[:2]
    mix_scratch = rest[2:21]
    moe_scratch = rest[21:32]
    arrived = rest[32]
    mix_sems = rest[33:49]
    moe_sems = rest[49:65]
    my = lax.axis_index("tp")
    me = lax.axis_index("sp")
    own = settled.shape[0]
    names = (
        "qa", "ka", "va", "ga", "da", "qb", "kb", "vb", "gb", "db", "pa", "pb", "stream", "wg", "wu", "wd",
    )
    place = {name: i for i, name in enumerate(names)}

    def load(name):
        i = place[name]
        src = hbm[i]
        if name == "stream":
            src = src.at[pl.ds(pl.multiple_of(my * own, own), own), :]
        return pltpu.make_async_copy(src, held[i], arrived.at[i])

    stages = [["da", "ka", "va"], ["db", "kb", "vb"], ["qa", "qb"], ["ga", "gb", "pa", "pb", "stream"]]
    for stage in stages:
        for name in stage:
            load(name).start()
    barrier = pltpu.get_barrier_semaphore()
    peers = [{"sp": lax.rem(me + k, n)} for k in range(1, n)] + [{"tp": lax.rem(my + k, m)} for k in range(1, m)]
    for peer in peers:
        pl.semaphore_signal(barrier, inc=1, device_id=peer, device_id_type=MESH)

    def start():
        pl.semaphore_wait(barrier, len(peers))
        for name in ("wg", "wu", "wd"):
            load(name).start()

    def ready(stage):
        for name in stages[stage]:
            load(name).wait()
        if stage == 2:
            for name in ("ga", "gb"):
                load(name).wait()
            stages[3] = [name for name in stages[3] if name not in ("ga", "gb")]

    mixer(n, m, held[:13], mix_scratch, ((start, ready),) + mix_sems, gain, gain_mix, columns, settled)
    experts_phase(
        n, m, capacity, routes, affinity, columns, settled, gain_moe, [load(w) for w in ("wg", "wu", "wd")],
        out, held[13:] + moe_scratch, moe_sems,
    )


def body(
    query_one,
    key_one,
    value_one,
    gate_one,
    decay_one,
    query_two,
    key_two,
    value_two,
    gate_two,
    decay_two,
    head_gain,
    proj_one,
    proj_two,
    stream,
    gain_mix,
    gain_moe,
    routes,
    affinity,
    expert_gate,
    expert_up,
    expert_down,
):
    shape = jax.ShapeDtypeStruct
    rows = query_one.shape[0]
    n = lax.axis_size("sp")
    m = lax.axis_size("tp")
    width = stream.shape[1]
    own = rows // m
    wide = width // m
    dv = head_gain.shape[0]
    lanes = query_one.shape[1] + query_two.shape[1]
    values = value_one.shape[1] + value_two.shape[1]
    local_experts = expert_gate.shape[0]
    experts = local_experts * n
    top = routes.shape[1]
    capacity = 3 * rows * top // (2 * experts)
    room = local_experts * capacity

    half = dv // 2
    pairs = n // 2
    lines = m // 2
    chunk = 128 if query_one.shape[1] % 128 == 0 and query_two.shape[1] % 128 == 0 else lanes
    chunks = lanes // chunk
    tiles = max(1, width // 512)
    vmem = pltpu.VMEM
    tall = vmem((n, lines, room, wide), BF16)
    flat = vmem((n, room, wide), BF16)
    whole = vmem((n, room, width), BF16)
    hbm = pl.BlockSpec(memory_space=pl.ANY)
    arrays = [
        query_one, key_one, value_one, gate_one, decay_one, query_two, key_two, value_two, gate_two, decay_two,
        proj_one, proj_two, stream, expert_gate, expert_up, expert_down,
    ]
    held = [vmem((own, width) if a is stream else a.shape, a.dtype) for a in arrays]
    mix_scratch = [
        vmem((2, 2, half, lanes), BF16), vmem((2, half, lanes), BF16), vmem((2, half, lanes), BF16),
        vmem((pairs, half, lanes), BF16), vmem((2, half, lanes), BF16), vmem((2, 2, half, lanes), BF16),
        vmem((2, 1, lanes), F32), vmem((2, 1, lanes), F32), vmem((2, 1, lanes), F32), vmem((pairs, 1, lanes), F32),
        vmem((2, rows, lanes), F32), vmem((rows, values), F32), vmem((2, rows, lanes), BF16),
        vmem((rows, values), BF16),
        vmem((rows, width), BF16), vmem((lines, own, width), BF16), vmem((lines, own, width), BF16),
        vmem((lines, own, width), BF16), vmem((own, width), BF16),
    ]
    moe_scratch = [
        flat, whole, whole, tall, tall, tall, flat, flat,
        vmem((rows, wide), F32), vmem((rows, wide), BF16), vmem((own, width), BF16),
    ]
    mix_sems = [
        DMA((chunks,)), DMA((chunks,)), DMA((chunks,)), DMA((chunks,)),
        DMA((chunks, pairs)), DMA((chunks, pairs)), DMA((chunks, pairs)), DMA((chunks, pairs)),
        DMA((chunks,)), DMA((chunks,)),
        DMA((lines, tiles)), DMA((lines, tiles)), DMA((lines, tiles)), DMA((lines, tiles)),
        DMA((m,)), DMA((m,)),
    ]
    moe_sems = [
        DMA((n,)), DMA((n,)), DMA((n, lines)), DMA((n, lines)), DMA((n,)), DMA((n,)),
        DMA((n, lines)), DMA((n, lines)), DMA((n, lines)), DMA((n, lines)), DMA((n, lines)), DMA((n, lines)),
        DMA((n,)), DMA((n,)), DMA((m,)), DMA((m,)),
    ]
    return pl.pallas_call(
        functools.partial(layer_kernel, n, m, capacity),
        out_shape=shape((own, width), BF16),
        in_specs=[VMEM] * 5 + [hbm] * len(arrays),
        out_specs=VMEM,
        scratch_shapes=held
        + [vmem((rows, wide), BF16), vmem((own, width), F32)]
        + mix_scratch + moe_scratch + [DMA((len(arrays),))] + mix_sems + moe_sems,
        compiler_params=params(1),
    )(
        routes.T, affinity.T, head_gain.reshape(1, -1), gain_mix.reshape(1, -1), gain_moe.reshape(1, -1), *arrays
    )


def solution(mesh):
    return jax.shard_map(
        body,
        mesh=mesh,
        in_specs=(
            P("sp", "tp"),
            P("sp", "tp"),
            P("sp", "tp"),
            P("sp", "tp"),
            P(None, "sp", "tp"),
            P("sp", "tp"),
            P("sp", "tp"),
            P("sp", "tp"),
            P("sp", "tp"),
            P(None, "sp", "tp"),
            P(),
            P("tp", None),
            P("tp", None),
            P("sp", None),
            P(),
            P(),
            P("sp", None),
            P("sp", None),
            P("sp", None, "tp"),
            P("sp", None, "tp"),
            P("sp", "tp", None),
        ),
        out_specs=P(("sp", "tp"), None),
        check_vma=False,
    )
```

time: 119 us -> 93.8 us (0.79)
  Pallas kernels: 111 us -> 91.9 us
  local copies, waits for them, and re-layouts: 6.81 us -> 1.67 us
    pallas_call x5 -> x1, Pallas kernels: 111 us -> 91.9 us  [body(): pl.pallas_call(functools.partial(layer_kernel, n, m, capacity), out_shape...]
    unnamed x41 -> x1, local copies, waits for them, and re-layouts: 6.81 us -> 1.67 us
where the time goes in v2:
time: 93.8 us; the launch traced here: 93.6 us
  Pallas kernels  91.9 us (98%)
  local copies, waits for them, and re-layouts  1.67 us (2%)
    pallas_call x1, Pallas kernels, body(): pl.pallas_call(functools.partial(layer_kernel, n, m, capacity), out_shape...  91.9 us

profile of v2, /device:TPU:1, one launch (start us, length us, event | category | flops | bytes accessed | tf_op | source)
XLA Modules:
  0.0 93.6 jit_solution(3234595569673969565)
XLA Ops:
  0.0 91.9 %shard_map.199 = bf16[64,2048]{1,0:T(8,128)(2,1)} custom-call(s32[2,256]{1,0:T(2,128)} %bitcast.7, f32[2,256]{1,0:T(2,128)} %bitcast.8, f32[1,128]{1,0:T(1,128)} %bitcast.9, f32[1,2048]{1,0:T(1,128)} %bitcast.5, f32[1,2048]{1,0:T(1,128)} %bitcast.6, bf16[256,256]{1,0:T(8,128)(2,1)} %refs_5_.1, bf16[256,256]{1,0:T(8,128)(2,1)} %refs_6_.1, ...), custom_call_target="tpu_custom_call" | custom-call | tf_op jit(solution)/shard_map/pallas_call | solution.py:799
  91.9 1.7 %copy.23 = bf16[64,2048]{1,0:T(8,128)(2,1)} copy(bf16[64,2048]{1,0:T(8,128)(2,1)} %shard_map.199) | data formatting | bytes 524288
